TPU v7x, 32 devices: a whole 2x2x4 slice. The times are simulated.
32 devices in a mesh: sp: 8 (over z, y), tp: 4 (over x, core).
Axes of the slice: x: 2, y: 2, z: 4, core: 2. Of those that a mesh axis runs over, the one named last changes fastest.
Arguments:
- queries: bfloat16 [2304, 2048], P('sp', 'tp'), as said below
- key_vectors: bfloat16 [2304, 2048], P('sp', 'tp'), as said below
- latents: bfloat16 [2304, 2048], P('sp'), as said below
- value_weight: bfloat16 [2048, 2048], P(None, 'tp'), as said below
- log_sums: float32 [2304, 32], P('sp', 'tp'), as said below
- out_first: bfloat16 [2304, 2048], P('sp', 'tp'), as said below
- out_second: bfloat16 [2304, 2048], P('sp', 'tp'), as said below
- cotangent: bfloat16 [2304, 2048], P('sp', 'tp'), may hold values from -6 to 6
- head_lambda: float32 [16], P('tp'), may hold values from 0.3 to 0.8
Outputs:
- grad_queries: float32 [2304, 2048], P('sp', 'tp')
- grad_keys: float32 [2304, 2048], P('sp', 'tp')
- grad_latents: bfloat16 [2304, 2048], P('sp', 'tp')
- grad_weight: float32 [2048, 2048], P('sp', 'tp')
Inputs may be any that keep to these rules, and one draw needn't show every extreme that they name: queries with entries of standard deviation 1.75. `key_vectors`: keys with entries of standard deviation 1. `latents`: inputs of standard deviation 1. `value_weight`: weights scaled by the inverse square root of 2048. `log_sums`: each row's log-sum of exponentials of its causal scores, for the given queries and keys. `out_first`: the first map's attention output for the given queries, keys, values and log-sums. `out_second`: the second map's attention output, likewise.
All inputs are finite; a program needn't handle non-finite values.
Results may differ from a plain program's by a relative error of at most 0.022.
Values may be sent and summed in bfloat16 or wider, within the bound.
A program may use at most 192 MiB of HBM per device.

v0:
```python
import functools

import jax
import jax.numpy as jnp
from jax import lax
from jax.experimental import pallas as pl
from jax.experimental.pallas import tpu as pltpu
from jax.sharding import PartitionSpec as P

DH = 64
DV = 128
BLOCK = 256


def row_terms(out_first, out_second, cotangent, head_lambda):
    count = out_first.shape[0]
    head_count = head_lambda.shape[0]
    first = out_first.astype(jnp.float32).reshape(count, head_count, DV)
    second = out_second.astype(jnp.float32).reshape(count, head_count, DV)
    mixed = first - head_lambda[None, :, None] * second
    inverse = lax.rsqrt(jnp.mean(mixed * mixed, axis=-1, keepdims=True) + 1e-06)
    normed = mixed * inverse
    grad_out = cotangent.astype(jnp.float32).reshape(count, head_count, DV)
    grad_mixed = inverse * (grad_out - normed * jnp.mean(grad_out * normed, axis=-1, keepdims=True))
    grad_rows = grad_mixed.astype(jnp.bfloat16)
    widened = lax.optimization_barrier(grad_rows).astype(jnp.float32)
    row_dots = jnp.stack(
        [jnp.sum(widened * first, axis=-1), jnp.sum(widened * second, axis=-1)], axis=-1
    )
    return (grad_rows.reshape(count, head_count * DV), row_dots.reshape(count, head_count * 2))


def block_grads(
    query_rows, grad_rows, lse_rows, dot_rows, query_pos, key_rows, value_rows, key_pos, head_lambda
):
    count = query_rows.shape[0]
    width = key_rows.shape[0]
    head_count = head_lambda.shape[0]
    score_scale = DH ** (-0.5)
    query_heads = query_rows.reshape(count, head_count, 2, DH)
    key_heads = key_rows.reshape(width, head_count, 2, DH)
    grad_heads = grad_rows.reshape(count, head_count, DV)
    value_heads = value_rows.reshape(width, head_count, DV)
    scores = (
        jnp.einsum("nhad,mhad->hanm", query_heads, key_heads, preferred_element_type=jnp.float32)
        * score_scale
    )
    causal = query_pos[:, None] >= key_pos[None, :]
    shifts = lse_rows.reshape(count, head_count, 2).transpose(1, 2, 0)[..., None]
    probs = jnp.exp(jnp.where(causal, scores - shifts, -1e30))
    d_attn = jnp.einsum("nhe,mhe->hnm", grad_heads, value_heads, preferred_element_type=jnp.float32)
    dots = dot_rows.reshape(count, head_count, 2).transpose(1, 2, 0)[..., None]
    map_weight = jnp.stack([jnp.ones_like(head_lambda), -head_lambda], axis=1)[:, :, None, None]
    d_scores = (map_weight * probs * (d_attn[:, None] - dots)).astype(jnp.bfloat16)
    weights = (probs[:, 0] - head_lambda[:, None, None] * probs[:, 1]).astype(jnp.bfloat16)
    grad_q = (
        jnp.einsum("hanm,mhad->nhad", d_scores, key_heads, preferred_element_type=jnp.float32)
        * score_scale
    )
    grad_k = (
        jnp.einsum("hanm,nhad->mhad", d_scores, query_heads, preferred_element_type=jnp.float32)
        * score_scale
    )
    grad_v = jnp.einsum("hnm,nhe->mhe", weights, grad_heads, preferred_element_type=jnp.float32)
    return (grad_q.reshape(count, -1), grad_k.reshape(width, -1), grad_v.reshape(width, -1))


def per_device(
    queries,
    key_vectors,
    latents,
    value_weight,
    log_sums,
    out_first,
    out_second,
    cotangent,
    head_lambda,
):
    local_rows = queries.shape[0]
    offset = lax.axis_index("sp") * local_rows
    positions = offset + jnp.arange(local_rows, dtype=jnp.int32)
    last_row = offset + local_rows - 1
    values = jnp.dot(latents, value_weight, preferred_element_type=jnp.float32).astype(jnp.bfloat16)
    grad_rows, row_dots = row_terms(out_first, out_second, cotangent, head_lambda)
    gathered_stats = (
        lax.all_gather(log_sums, "sp", axis=0, tiled=True),
        lax.all_gather(row_dots, "sp", axis=0, tiled=True),
    )
    key_rows = lax.all_gather(key_vectors, "sp", axis=0, tiled=True)
    value_rows = lax.all_gather(values, "sp", axis=0, tiled=True)
    count = key_rows.shape[0]

    def compute(current):
        key_pos = jnp.arange(count, dtype=jnp.int32)
        grad_q, unused_k, unused_v = block_grads(
            queries,
            grad_rows,
            log_sums,
            row_dots,
            positions,
            key_rows,
            value_rows,
            key_pos,
            head_lambda,
        )
        return grad_q

    grad_queries = lax.cond(
        jnp.int32(0) <= last_row,
        compute,
        lambda current: current,
        jnp.zeros((local_rows, queries.shape[1]), jnp.float32),
    )
    start_totals = (
        jnp.zeros((local_rows, key_vectors.shape[1]), jnp.float32),
        jnp.zeros((local_rows, values.shape[1]), jnp.float32),
    )
    query_rows = lax.all_gather(queries, "sp", axis=0, tiled=True)
    grad_piece = lax.all_gather(grad_rows, "sp", axis=0, tiled=True)
    add_count = query_rows.shape[0]

    def compute(current):
        query_pos = jnp.arange(add_count, dtype=jnp.int32)
        lse_rows = gathered_stats[0]
        dot_rows = gathered_stats[1]
        unused_q, grad_k, grad_v = block_grads(
            query_rows,
            grad_piece,
            lse_rows,
            dot_rows,
            query_pos,
            key_vectors,
            values,
            positions,
            head_lambda,
        )
        return (grad_k, grad_v)

    grad_keys, grad_values = lax.cond(
        jnp.int32(0) + add_count - 1 >= offset, compute, lambda current: current, start_totals
    )
    values_grad = grad_values.astype(jnp.bfloat16)
    grad_weight = lax.psum_scatter(
        lax.dot_general(
            latents, values_grad, (((0,), (0,)), ((), ())), preferred_element_type=jnp.float32
        ).astype(jnp.bfloat16),
        "sp",
        scatter_dimension=0,
        tiled=True,
    ).astype(jnp.float32)
    latent_partial = lax.dot_general(
        values_grad, value_weight, (((1,), (1,)), ((), ())), preferred_element_type=jnp.float32
    )
    grad_latents = lax.psum_scatter(
        latent_partial.astype(jnp.bfloat16), "tp", scatter_dimension=1, tiled=True
    )
    return (grad_queries, grad_keys, grad_latents, grad_weight)


def exchange_kernel(axis, n, parts, *refs):
    swap_blocks(axis, n, refs[:parts], refs[parts : 2 * parts], *refs[2 * parts :])


def swap_blocks(axis, n, ins, outs, send_sem, recv_sem, local_sem, prepare=lambda: None):
    parts = len(ins)
    me = lax.axis_index(axis)
    barrier = pltpu.get_barrier_semaphore()
    for step in range(1, n):
        peer = lax.rem(me + step, n)
        pl.semaphore_signal(
            barrier, inc=1, device_id={axis: peer}, device_id_type=pl.DeviceIdType.MESH
        )
    prepare()
    pl.semaphore_wait(barrier, n - 1)

    def remote(part, step, slot):
        peer = lax.rem(me + step, n)
        return pltpu.make_async_remote_copy(
            src_ref=ins[part].at[peer],
            dst_ref=outs[part].at[slot],
            send_sem=send_sem.at[part, step],
            recv_sem=recv_sem.at[part, step],
            device_id={axis: peer},
            device_id_type=pl.DeviceIdType.MESH,
        )

    order = sorted(range(1, n), key=lambda step: -min(step, n - step))
    for part in reversed(range(parts)):
        for step in order:
            remote(part, step, me).start()
    for part in range(parts):
        own = pltpu.make_async_copy(ins[part].at[me], outs[part].at[me], local_sem.at[part])
        own.start()
        own.wait()
    for part in range(parts):
        for step in order:
            remote(part, step, lax.rem(me + n - step, n)).wait_recv()
    for part in range(parts):
        for step in order:
            remote(part, step, me).wait_send()


def exchange(arrays, axis, n, collective_id):
    parts = len(arrays)
    sent = sum(a.size * a.dtype.itemsize for a in arrays)
    return pl.pallas_call(
        functools.partial(exchange_kernel, axis, n, parts),
        out_shape=[jax.ShapeDtypeStruct(a.shape, a.dtype) for a in arrays],
        in_specs=[pl.BlockSpec(memory_space=pltpu.VMEM)] * parts,
        out_specs=[pl.BlockSpec(memory_space=pltpu.VMEM)] * parts,
        scratch_shapes=[
            pltpu.SemaphoreType.DMA((parts, n)),
            pltpu.SemaphoreType.DMA((parts, n)),
            pltpu.SemaphoreType.DMA((parts,)),
        ],
        compiler_params=pltpu.CompilerParams(collective_id=collective_id, has_side_effects=True),
        cost_estimate=pl.CostEstimate(flops=0, bytes_accessed=sent * 16, transcendentals=0),
    )(*arrays)


def head_of(index):
    return slice(index * DV, (index + 1) * DV)


def send_kernel(
    axis, n, q_ref, k_ref, v_ref, first_ref, second_ref, cot_ref, lse_ref, lambda_ref,
    x_out, stats_out, x_s, stats_s, *sems
):
    def prepare():
        score_scale = jnp.bfloat16(DH**-0.5)
        columns = []
        stats_s[...] = jnp.zeros_like(stats_s)
        for head in range(n // 2):
            lanes = head_of(head)
            first = first_ref[:, lanes].astype(jnp.float32)
            second = second_ref[:, lanes].astype(jnp.float32)
            mixed = first - lambda_ref[head] * second
            inverse = lax.rsqrt(jnp.mean(mixed * mixed, axis=-1, keepdims=True) + 1e-06)
            normed = mixed * inverse
            grad_out = cot_ref[:, lanes].astype(jnp.float32)
            mean_dot = jnp.mean(grad_out * normed, axis=-1, keepdims=True)
            grad_rows = (inverse * (grad_out - normed * mean_dot)).astype(jnp.bfloat16)
            widened = grad_rows.astype(jnp.float32)
            columns.append(jnp.sum(widened * first, axis=-1, keepdims=True))
            columns.append(jnp.sum(widened * second, axis=-1, keepdims=True))
            q_pair = q_ref[:, lanes] * score_scale
            k_pair = k_ref[:, lanes]
            for m in range(2):
                unit = 2 * head + m
                half = slice(m * DH, (m + 1) * DH)
                x_s[unit, :, 0 : 2 * DH] = jnp.concatenate(
                    [q_pair[:, half], k_pair[:, half]], axis=1
                )
                x_s[unit, :, 2 * DH : 2 * DH + DV] = v_ref[:, lanes]
                x_s[unit, :, 2 * DH + DV :] = grad_rows
        dots = jnp.concatenate(columns, axis=1).T
        for unit in range(n):
            stats_s[unit, 0:1, :] = lse_ref[unit : unit + 1, :]
            stats_s[unit, 1:2, :] = dots[unit : unit + 1, :]

    swap_blocks(axis, n, (x_s, stats_s), (x_out, stats_out), *sems, prepare=prepare)


def send_units(queries, keys, values, first, second, cotangent, lse, head_lambda, n):
    rows = queries.shape[0]
    shapes = [((n, rows, 2 * DH + 2 * DV), jnp.bfloat16), ((n, 8, rows), jnp.float32)]
    vmem = pl.BlockSpec(memory_space=pltpu.VMEM)
    return pl.pallas_call(
        functools.partial(send_kernel, "sp", n),
        out_shape=[jax.ShapeDtypeStruct(*shape) for shape in shapes],
        in_specs=[vmem] * 7 + [pl.BlockSpec(memory_space=pltpu.SMEM)],
        out_specs=[vmem] * 2,
        scratch_shapes=[pltpu.VMEM(*shape) for shape in shapes]
        + [
            pltpu.SemaphoreType.DMA((2, n)),
            pltpu.SemaphoreType.DMA((2, n)),
            pltpu.SemaphoreType.DMA((2,)),
        ],
        compiler_params=pltpu.CompilerParams(collective_id=1, has_side_effects=True),
        cost_estimate=pl.CostEstimate(
            flops=0, bytes_accessed=queries.size * 64, transcendentals=0
        ),
    )(queries, keys, values, first, second, cotangent, lse, head_lambda)


def unpack_kernel(x_ref, lambda_ref, q_ref, k_ref, v_ref):
    for head in range(x_ref.shape[0] // 2):
        lanes = head_of(head)
        weight = -lambda_ref[head]
        first = x_ref[2 * head].astype(jnp.float32)
        second = x_ref[2 * head + 1].astype(jnp.float32) * weight
        q_ref[:, lanes] = jnp.concatenate([first[:, :DH], second[:, :DH]], axis=1) * DH ** (-0.5)
        k_ref[:, lanes] = jnp.concatenate(
            [first[:, DH : 2 * DH], second[:, DH : 2 * DH]], axis=1
        )
        v_ref[:, lanes] = (first[:, 2 * DH :] + second[:, 2 * DH :]).astype(jnp.bfloat16)


def unpack(grads, head_lambda):
    n, rows, _ = grads.shape
    vmem = pl.BlockSpec(memory_space=pltpu.VMEM)
    kinds = (jnp.float32, jnp.float32, jnp.bfloat16)
    return pl.pallas_call(
        unpack_kernel,
        out_shape=[jax.ShapeDtypeStruct((rows, n * DH), kind) for kind in kinds],
        in_specs=[vmem, pl.BlockSpec(memory_space=pltpu.SMEM)],
        out_specs=[vmem] * 3,
        cost_estimate=pl.CostEstimate(flops=0, bytes_accessed=grads.size * 6, transcendentals=0),
    )(grads, head_lambda)


def attention_kernel(block, x_ref, stats_ref, o_ref, q_s, k_s, kt_s, dqt_s, dk_s, dv_s):
    blocks = x_ref.shape[0] // block

    def rows_of(index):
        return pl.ds(pl.multiple_of(index * block, block), block)

    def prologue(index, carry):
        rows = rows_of(index)
        pair = x_ref[rows, 0 : 2 * DH]
        q_s[rows, :] = pair[:, :DH]
        keys = pair[:, DH:]
        k_s[rows, :] = keys
        kt_s[index] = keys.T
        dqt_s[index] = jnp.zeros((DH, block), jnp.float32)
        return carry

    lax.fori_loop(0, blocks, prologue, 0)

    def tile(key_index, query_index, diagonal):
        key_rows, query_rows = rows_of(key_index), rows_of(query_index)
        queries = q_s[query_rows, :]
        grads = x_ref[query_rows, 2 * DH + DV :]
        nt = (((1,), (1,)), ((), ()))
        scores = lax.dot_general(
            k_s[key_rows, :], queries, nt, preferred_element_type=jnp.float32
        )
        stats = stats_ref[query_index]
        shifted = scores - stats[0:1, :]
        if diagonal:
            key_at = lax.broadcasted_iota(jnp.int32, (block, block), 0)
            query_at = lax.broadcasted_iota(jnp.int32, (block, block), 1)
            shifted = jnp.where(query_at >= key_at, shifted, -1e30)
        probs = jnp.exp(shifted)
        d_attn = lax.dot_general(
            x_ref[key_rows, 2 * DH : 2 * DH + DV], grads, nt, preferred_element_type=jnp.float32
        )
        d_scores = (probs * (d_attn - stats[1:2, :])).astype(jnp.bfloat16)
        weights = probs.astype(jnp.bfloat16)
        dk = jnp.dot(d_scores, queries, preferred_element_type=jnp.float32)
        dv = jnp.dot(weights, grads, preferred_element_type=jnp.float32)
        dqt_s[query_index] += jnp.dot(
            kt_s[key_index], d_scores, preferred_element_type=jnp.float32
        )
        if diagonal:
            dk_s[...] = dk
            dv_s[...] = dv
        else:
            dk_s[...] += dk
            dv_s[...] += dv

    def column(key_index, carry):
        tile(key_index, key_index, True)

        def inner(query_index, carry):
            tile(key_index, query_index, False)
            return carry

        lax.fori_loop(key_index + 1, blocks, inner, 0)
        out = [dqt_s[key_index].T, dk_s[...], dv_s[...]]
        o_ref[rows_of(key_index), :] = jnp.concatenate(out, axis=1).astype(jnp.bfloat16)
        return carry

    lax.fori_loop(0, blocks, column, 0)


def attention(x, stats, block):
    count = x.shape[0]
    pairs = count * (count + block) // 2
    return pl.pallas_call(
        functools.partial(attention_kernel, block),
        out_shape=jax.ShapeDtypeStruct((count, 2 * DH + DV), jnp.bfloat16),
        in_specs=[pl.BlockSpec(memory_space=pltpu.VMEM)] * 2,
        out_specs=pl.BlockSpec(memory_space=pltpu.VMEM),
        scratch_shapes=[
            pltpu.VMEM((count, DH), jnp.bfloat16),
            pltpu.VMEM((count, DH), jnp.bfloat16),
            pltpu.VMEM((count // block, DH, block), jnp.bfloat16),
            pltpu.VMEM((count // block, DH, block), jnp.float32),
            pltpu.VMEM((block, DH), jnp.float32),
            pltpu.VMEM((block, DV), jnp.float32),
        ],
        cost_estimate=pl.CostEstimate(
            flops=2 * pairs * 448, bytes_accessed=count * 1600, transcendentals=pairs
        ),
    )(x, stats)


def weight_kernel(
    axis, n, lat_ref, dv_ref, o_ref, to_pair, from_pair, sums, from_line,
    pair_send, pair_recv, line_send, line_recv
):
    line = n // 2
    me = lax.axis_index(axis)
    place, side = me // 2, lax.rem(me, 2)
    partner = 2 * place + 1 - side
    width = lat_ref.shape[1] // n
    mesh_id = pl.DeviceIdType.MESH

    def at(step):
        return lax.rem(place + step, line)

    def term(unit):
        columns = pl.ds(pl.multiple_of(unit * width, width), width)
        return lax.dot_general(
            lat_ref[:, columns],
            dv_ref[...],
            (((0,), (0,)), ((), ())),
            preferred_element_type=jnp.float32,
        )

    def pair_copy(step):
        return pltpu.make_async_remote_copy(
            src_ref=to_pair.at[step],
            dst_ref=from_pair.at[step],
            send_sem=pair_send.at[step],
            recv_sem=pair_recv.at[step],
            device_id={axis: partner},
            device_id_type=mesh_id,
        )

    def line_copy(step):
        return pltpu.make_async_remote_copy(
            src_ref=sums.at[step],
            dst_ref=from_line.at[step],
            send_sem=line_send.at[step],
            recv_sem=line_recv.at[step],
            device_id={axis: 2 * at(step) + side},
            device_id_type=mesh_id,
        )

    barrier = pltpu.get_barrier_semaphore()
    pl.semaphore_signal(barrier, inc=1, device_id={axis: partner}, device_id_type=mesh_id)
    for step in range(1, line):
        pl.semaphore_signal(
            barrier, inc=1, device_id={axis: 2 * at(step) + side}, device_id_type=mesh_id
        )
    order = sorted(range(1, line), key=lambda step: -min(step, line - step)) + [0]
    to_pair[order[0]] = term(2 * at(order[0]) + 1 - side).astype(jnp.bfloat16)
    pl.semaphore_wait(barrier, line)
    pair_copy(order[0]).start()
    for step in order[1:]:
        to_pair[step] = term(2 * at(step) + 1 - side).astype(jnp.bfloat16)
        pair_copy(step).start()
    for step in order:
        own = term(2 * at(step) + side)
        pair_copy(step).wait_recv()
        total = own + from_pair[step].astype(jnp.float32)
        if step == 0:
            o_ref[...] = total
        else:
            sums[step] = total.astype(jnp.bfloat16)
            line_copy(step).start()
    for step in order[:-1]:
        line_copy(step).wait_recv()
        o_ref[...] += from_line[step].astype(jnp.float32)
    for step in order:
        pair_copy(step).wait_send()
    for step in order[:-1]:
        line_copy(step).wait_send()


def summed_weight(latents, values_grad, n):
    rows, depth = latents.shape
    columns = values_grad.shape[1]
    width = depth // n
    vmem = pl.BlockSpec(memory_space=pltpu.VMEM)
    buffer = pltpu.VMEM((n // 2, width, columns), jnp.bfloat16)
    return pl.pallas_call(
        functools.partial(weight_kernel, "sp", n),
        out_shape=jax.ShapeDtypeStruct((width, columns), jnp.float32),
        in_specs=[vmem] * 2,
        out_specs=vmem,
        scratch_shapes=[buffer] * 4 + [pltpu.SemaphoreType.DMA((n // 2,))] * 4,
        compiler_params=pltpu.CompilerParams(collective_id=3, has_side_effects=True),
        cost_estimate=pl.CostEstimate(
            flops=2 * rows * depth * columns,
            bytes_accessed=depth * columns * 64,
            transcendentals=0,
        ),
    )(latents, values_grad)


def by_unit(
    queries,
    key_vectors,
    latents,
    value_weight,
    log_sums,
    out_first,
    out_second,
    cotangent,
    head_lambda,
):
    n = lax.axis_size("sp")
    rows = queries.shape[0]
    values = jnp.dot(latents, value_weight, preferred_element_type=jnp.float32).astype(jnp.bfloat16)
    packed, stats = send_units(
        queries, key_vectors, values, out_first, out_second, cotangent, log_sums.T, head_lambda, n
    )
    count = n * rows
    stats = stats.transpose(1, 0, 2).reshape(8, count // BLOCK, BLOCK).transpose(1, 0, 2)
    grads = attention(packed.reshape(count, 2 * DH + 2 * DV), stats, BLOCK)
    (grads,) = exchange([grads.reshape(n, rows, 2 * DH + DV)], "sp", n, 2)
    grad_queries, grad_keys, values_grad = unpack(grads, head_lambda)
    latent_partial = lax.dot_general(
        values_grad, value_weight, (((1,), (1,)), ((), ())), preferred_element_type=jnp.float32
    )
    grad_latents = lax.psum_scatter(
        latent_partial.astype(jnp.bfloat16), "tp", scatter_dimension=1, tiled=True
    )
    grad_weight = summed_weight(latents, values_grad, n)
    return (grad_queries, grad_keys, grad_latents, grad_weight)


def dispatch(queries, key_vectors, latents, value_weight, log_sums, *rest):
    n = lax.axis_size("sp")
    count = n * queries.shape[0]
    fits = rest[-1].shape[0] * 2 == n and count % BLOCK == 0
    fits = fits and latents.shape[1] % (n * DV) == 0
    run = by_unit if fits else per_device
    return run(queries, key_vectors, latents, value_weight, log_sums, *rest)


def solution(mesh):
    return jax.shard_map(
        dispatch,
        mesh=mesh,
        in_specs=(
            P("sp", "tp"),
            P("sp", "tp"),
            P("sp", None),
            P(None, "tp"),
            P("sp", "tp"),
            P("sp", "tp"),
            P("sp", "tp"),
            P("sp", "tp"),
            P("tp"),
        ),
        out_specs=(P("sp", "tp"), P("sp", "tp"), P("sp", "tp"), P("sp", "tp")),
        check_vma=False,
    )
```

profile of v0, /device:TPU:0, one launch (start us, length us, event | category | flops | bytes accessed | tf_op | source)
XLA Modules:
  0.0 163.9 jit_solution(11001234912498826628)
XLA Ops:
  7.2 0.0 copy-start
  7.2 0.0 reduce-scatter.2.cloned.1.call-start
  7.2 1.5 copy-done
  8.8 2.8 %convolution_convert_fusion.1.v_ref = bf16[288,512]{1,0:T(8,128)(2,1)} fusion(bf16[288,2048]{1,0:T(8,128)(2,1)} %lat_ref.1, bf16[2048,512]{1,0:T(8,128)(2,1)S(1)} %copy-done), kind=kOutput, calls=%fused_computation.1 | convolution fusion | flops 604127232 | bytes 3571712 | tf_op jit(solution)/shard_map/dot_general | solution.py:507
  11.5 42.0 %shard_map.120 = (bf16[8,288,384]{2,1,0:T(8,128)(2,1)}, f32[8,8,288]{2,1,0:T(8,128)}) custom-call(bf16[288,512]{1,0:T(8,128)(2,1)} %q_ref.1, bf16[288,512]{1,0:T(8,128)(2,1)} %k_ref.1, bf16[288,512]{1,0:T(8,128)(2,1)} %convolution_convert_fusion.1.v_ref, bf16[288,512]{1,0:T(8,128)(2,1)} %first_ref.1, bf16[288,512]{1,0:T(8,128)(2,1)} %second_ref.1, ...), custom_call_target="tpu_custom_call" | custom-call | bytes 9437184 | tf_op jit(solution)/shard_map/pallas_call | solution.py:268
  53.5 0.9 copy.13
  54.4 0.1 reshape.18
  54.5 0.7 copy.16
  55.2 22.2 %shard_map.121 = bf16[2304,256]{1,0:T(8,128)(2,1)} custom-call(bf16[2304,384]{1,0:T(8,128)(2,1)} %bitcast.15, f32[9,8,256]{2,1,0:T(8,128)} %bitcast.13), custom_call_target="tpu_custom_call" | custom-call | flops 2642411520 | bytes 3686400 | tf_op jit(solution)/shard_map/pallas_call | solution.py:380
  77.4 33.9 %shard_map.122.x_ref = bf16[8,288,256]{2,1,0:T(8,128)(2,1)} custom-call(bf16[8,288,256]{2,1,0:T(8,128)(2,1)} %bitcast.11), custom_call_target="tpu_custom_call" | custom-call | bytes 18874368 | tf_op jit(solution)/shard_map/pallas_call | solution.py:206
  111.3 2.7 %shard_map.123 = (f32[288,512]{1,0:T(8,128)}, f32[288,512]{1,0:T(8,128)}, bf16[288,512]{1,0:T(8,128)(2,1)}) custom-call(bf16[8,288,256]{2,1,0:T(8,128)(2,1)} %shard_map.122.x_ref, f32[4]{0:T(128)} %lambda_ref.3), custom_call_target="tpu_custom_call" | custom-call | bytes 3538944 | tf_op jit(solution)/shard_map/pallas_call | solution.py:303
  114.0 2.8 %convolution_convert_fusion = bf16[288,2048]{1,0:T(8,128)(2,1)} fusion(bf16[288,512]{1,0:T(8,128)(2,1)} %get-tuple-element.13.dv_ref, bf16[2048,512]{1,0:T(8,128)(2,1)S(1)} %copy-done), kind=kOutput, calls=%fused_computation | convolution fusion | flops 604569600 | bytes 3571712 | tf_op jit(solution)/shard_map/dot_general | solution.py:516
  116.8 0.0 reduce-scatter.2.cloned.1.call-update
  116.8 38.3 %shard_map.124 = f32[256,512]{1,0:T(8,128)} custom-call(bf16[288,2048]{1,0:T(8,128)(2,1)} %lat_ref.1, bf16[288,512]{1,0:T(8,128)(2,1)} %get-tuple-element.13.dv_ref), custom_call_target="tpu_custom_call" | custom-call | flops 603979776 | bytes 67108864 | tf_op jit(solution)/shard_map/pallas_call | solution.py:479
  155.1 0.0 reduce-scatter.2.cloned.1.call-done
  155.2 1.9 %copy.18 = f32[256,512]{1,0:T(8,128)} copy(f32[256,512]{1,0:T(8,128)} %shard_map.124) | data formatting | bytes 1048576
Async XLA Ops:
  7.2 1.6 copy-start
  7.2 148.0 %reduce-scatter.2.cloned.1.call-start = ((), (), s32[]{:S(2)}) async-start(), calls=%async_computation.1 | async-start | bytes 1474560 | tf_op jit(solution)/shard_map/reduce_scatter | solution.py:519
Sparse Core Ops, SparseCore 0:
  117.0 29.0 reduce-scatter.1
where the time goes:
time: 164 us
  Pallas kernels  139 us (85%)
  between operations  14.1 us (9%)
  matrix products  5.54 us (3%)
  local copies, waits for them, and re-layouts  5.11 us (3%)
    pallas_call x1, Pallas kernels, send_units(): pl.pallas_call(functools.partial(send_kernel, 'sp', n), out_shape=[jax.Sh...  42 us
    pallas_call x1, Pallas kernels, summed_weight(): pl.pallas_call(functools.partial(weight_kernel, 'sp', n), out_shape=jax.S...  38.3 us
    pallas_call x1, Pallas kernels, exchange(): pl.pallas_call(functools.partial(exchange_kernel, axis, n, parts), out_sh...  33.9 us
    pallas_call x1, Pallas kernels, attention(): pl.pallas_call(functools.partial(attention_kernel, block), out_shape=jax....  22.2 us
    unnamed x3, local copies, waits for them, and re-layouts  3.41 us
  transfers between devices with their start and end apart: 1, of which 0 were waited for; matrix products, arithmetic and copies ran while one was open for 0% of the time, Pallas kernels for 23%

commit v1 on v0

v1 whole, which is shorter than its diff:
```python
import functools

import jax
import jax.numpy as jnp
from jax import lax
from jax.experimental import pallas as pl
from jax.experimental.pallas import tpu as pltpu
from jax.sharding import PartitionSpec as P

DH = 64
DV = 128
BLOCK = 256


def row_terms(out_first, out_second, cotangent, head_lambda):
    count = out_first.shape[0]
    head_count = head_lambda.shape[0]
    first = out_first.astype(jnp.float32).reshape(count, head_count, DV)
    second = out_second.astype(jnp.float32).reshape(count, head_count, DV)
    mixed = first - head_lambda[None, :, None] * second
    inverse = lax.rsqrt(jnp.mean(mixed * mixed, axis=-1, keepdims=True) + 1e-06)
    normed = mixed * inverse
    grad_out = cotangent.astype(jnp.float32).reshape(count, head_count, DV)
    grad_mixed = inverse * (grad_out - normed * jnp.mean(grad_out * normed, axis=-1, keepdims=True))
    grad_rows = grad_mixed.astype(jnp.bfloat16)
    widened = lax.optimization_barrier(grad_rows).astype(jnp.float32)
    row_dots = jnp.stack(
        [jnp.sum(widened * first, axis=-1), jnp.sum(widened * second, axis=-1)], axis=-1
    )
    return (grad_rows.reshape(count, head_count * DV), row_dots.reshape(count, head_count * 2))


def block_grads(
    query_rows, grad_rows, lse_rows, dot_rows, query_pos, key_rows, value_rows, key_pos, head_lambda
):
    count = query_rows.shape[0]
    width = key_rows.shape[0]
    head_count = head_lambda.shape[0]
    score_scale = DH ** (-0.5)
    query_heads = query_rows.reshape(count, head_count, 2, DH)
    key_heads = key_rows.reshape(width, head_count, 2, DH)
    grad_heads = grad_rows.reshape(count, head_count, DV)
    value_heads = value_rows.reshape(width, head_count, DV)
    scores = (
        jnp.einsum("nhad,mhad->hanm", query_heads, key_heads, preferred_element_type=jnp.float32)
        * score_scale
    )
    causal = query_pos[:, None] >= key_pos[None, :]
    shifts = lse_rows.reshape(count, head_count, 2).transpose(1, 2, 0)[..., None]
    probs = jnp.exp(jnp.where(causal, scores - shifts, -1e30))
    d_attn = jnp.einsum("nhe,mhe->hnm", grad_heads, value_heads, preferred_element_type=jnp.float32)
    dots = dot_rows.reshape(count, head_count, 2).transpose(1, 2, 0)[..., None]
    map_weight = jnp.stack([jnp.ones_like(head_lambda), -head_lambda], axis=1)[:, :, None, None]
    d_scores = (map_weight * probs * (d_attn[:, None] - dots)).astype(jnp.bfloat16)
    weights = (probs[:, 0] - head_lambda[:, None, None] * probs[:, 1]).astype(jnp.bfloat16)
    grad_q = (
        jnp.einsum("hanm,mhad->nhad", d_scores, key_heads, preferred_element_type=jnp.float32)
        * score_scale
    )
    grad_k = (
        jnp.einsum("hanm,nhad->mhad", d_scores, query_heads, preferred_element_type=jnp.float32)
        * score_scale
    )
    grad_v = jnp.einsum("hnm,nhe->mhe", weights, grad_heads, preferred_element_type=jnp.float32)
    return (grad_q.reshape(count, -1), grad_k.reshape(width, -1), grad_v.reshape(width, -1))


def per_device(
    queries,
    key_vectors,
    latents,
    value_weight,
    log_sums,
    out_first,
    out_second,
    cotangent,
    head_lambda,
):
    local_rows = queries.shape[0]
    offset = lax.axis_index("sp") * local_rows
    positions = offset + jnp.arange(local_rows, dtype=jnp.int32)
    last_row = offset + local_rows - 1
    values = jnp.dot(latents, value_weight, preferred_element_type=jnp.float32).astype(jnp.bfloat16)
    grad_rows, row_dots = row_terms(out_first, out_second, cotangent, head_lambda)
    gathered_stats = (
        lax.all_gather(log_sums, "sp", axis=0, tiled=True),
        lax.all_gather(row_dots, "sp", axis=0, tiled=True),
    )
    key_rows = lax.all_gather(key_vectors, "sp", axis=0, tiled=True)
    value_rows = lax.all_gather(values, "sp", axis=0, tiled=True)
    count = key_rows.shape[0]

    def compute(current):
        key_pos = jnp.arange(count, dtype=jnp.int32)
        grad_q, unused_k, unused_v = block_grads(
            queries,
            grad_rows,
            log_sums,
            row_dots,
            positions,
            key_rows,
            value_rows,
            key_pos,
            head_lambda,
        )
        return grad_q

    grad_queries = lax.cond(
        jnp.int32(0) <= last_row,
        compute,
        lambda current: current,
        jnp.zeros((local_rows, queries.shape[1]), jnp.float32),
    )
    start_totals = (
        jnp.zeros((local_rows, key_vectors.shape[1]), jnp.float32),
        jnp.zeros((local_rows, values.shape[1]), jnp.float32),
    )
    query_rows = lax.all_gather(queries, "sp", axis=0, tiled=True)
    grad_piece = lax.all_gather(grad_rows, "sp", axis=0, tiled=True)
    add_count = query_rows.shape[0]

    def compute(current):
        query_pos = jnp.arange(add_count, dtype=jnp.int32)
        lse_rows = gathered_stats[0]
        dot_rows = gathered_stats[1]
        unused_q, grad_k, grad_v = block_grads(
            query_rows,
            grad_piece,
            lse_rows,
            dot_rows,
            query_pos,
            key_vectors,
            values,
            positions,
            head_lambda,
        )
        return (grad_k, grad_v)

    grad_keys, grad_values = lax.cond(
        jnp.int32(0) + add_count - 1 >= offset, compute, lambda current: current, start_totals
    )
    values_grad = grad_values.astype(jnp.bfloat16)
    grad_weight = lax.psum_scatter(
        lax.dot_general(
            latents, values_grad, (((0,), (0,)), ((), ())), preferred_element_type=jnp.float32
        ).astype(jnp.bfloat16),
        "sp",
        scatter_dimension=0,
        tiled=True,
    ).astype(jnp.float32)
    latent_partial = lax.dot_general(
        values_grad, value_weight, (((1,), (1,)), ((), ())), preferred_element_type=jnp.float32
    )
    grad_latents = lax.psum_scatter(
        latent_partial.astype(jnp.bfloat16), "tp", scatter_dimension=1, tiled=True
    )
    return (grad_queries, grad_keys, grad_latents, grad_weight)


def level(z, k, nz):
    bit, out = 1, z
    while bit < nz:
        out = out + ((k // bit) % 2) * bit * (1 - 2 * ((z // bit) % 2))
        bit *= 2
    return out


def lanes(index, width=DV):
    return pl.ds(pl.multiple_of(index * width, width), width)


def chunk(index, rows):
    return pl.ds(pl.multiple_of(index * rows, rows), rows)


def pad_tiles(rows, block=BLOCK):
    return -(-rows // block)


def remote(src, dst, send_sem, recv_sem, where):
    return pltpu.make_async_remote_copy(
        src_ref=src,
        dst_ref=dst,
        send_sem=send_sem,
        recv_sem=recv_sem,
        device_id=where,
        device_id_type=pl.DeviceIdType.MESH,
    )


def greet(devices):
    barrier = pltpu.get_barrier_semaphore()
    for device in devices:
        pl.semaphore_signal(
            barrier, inc=1, device_id=device, device_id_type=pl.DeviceIdType.MESH
        )
    return lambda: pl.semaphore_wait(barrier, len(devices))


NT = (((1,), (1,)), ((), ()))
TN = (((0,), (0,)), ((), ()))


def forward_kernel(
    nz, q_ref, k_ref, lat_ref, w_ref, first_ref, second_ref, cot_ref, lse_ref, lambda_ref,
    dq_ref, dkm_ref, dvm_ref, dko_ref, dvo_ref, latp_ref,
    first_s, second_s, cot_s, lat_s, w_s, grad_s, stat_s, v_s,
    q_all, do_all, k_all, v_all, stat_r, q0_s, q1_s, stat_t, dqt_s, dk_s, dv_s,
    load_sem, own_sem, send_sem, recv_sem, pass_send, pass_recv, lat_send, lat_recv
):
    sp = lax.axis_index("sp")
    z, y = sp // 2, lax.rem(sp, 2)
    rows = q_ref.shape[0]
    width = latp_ref.shape[2]
    tiles = stat_t.shape[0]
    partner = {"sp": 2 * z + 1 - y}
    peers = [{"sp": 2 * level(z, k, nz) + y} for k in range(1, nz)]
    loads = [
        pltpu.make_async_copy(src, dst, load_sem.at[i])
        for i, (src, dst) in enumerate(
            [(first_ref, first_s), (second_ref, second_s), (cot_ref, cot_s),
             (lat_ref, lat_s), (w_ref, w_s)]
        )
    ]
    for load in loads:
        load.start()
    arrived = greet(peers + [partner])
    own_q = pltpu.make_async_copy(q_ref.at[:, lanes(z)], q_all.at[chunk(z, rows)], own_sem.at[0])
    own_k = pltpu.make_async_copy(k_ref.at[:, lanes(z)], k_all.at[chunk(sp, rows)], own_sem.at[1])
    own_q.start()
    own_k.start()
    tail = q_all.shape[0] - nz * rows
    q_all[nz * rows :, :] = jnp.zeros((tail, DV), jnp.bfloat16)
    do_all[nz * rows :, :] = jnp.zeros((tail, DV), jnp.bfloat16)
    dqt_s[...] = jnp.zeros_like(dqt_s)
    arrived()

    def send(part, k):
        where = peers[k - 1]
        to = level(z, k, nz)
        src, dst = {
            0: (q_ref.at[:, lanes(to)], q_all.at[chunk(z, rows)]),
            1: (grad_s.at[:, lanes(to)], do_all.at[chunk(z, rows)]),
            2: (stat_s.at[to], stat_r.at[z]),
            3: (k_ref.at[:, lanes(to)], k_all.at[chunk(sp, rows)]),
            4: (v_s.at[:, lanes(to)], v_all.at[chunk(sp, rows)]),
        }[part]
        return remote(src, dst, send_sem.at[part, k], recv_sem.at[part, k], where)

    def passed(part, k, src, at):
        dst = (k_all, v_all)[part].at[chunk(at, rows)]
        return remote(src, dst, pass_send.at[part, k], pass_recv.at[part, k], partner)

    def lat_copy(t):
        return remote(
            lat_ref.at[:, lanes(2 * t + 1 - y, width)], latp_ref.at[t],
            lat_send.at[t], lat_recv.at[t], partner
        )

    for k in range(1, nz):
        send(0, k).start()
    passed(0, 0, k_ref.at[:, lanes(z)], sp).start()
    for t in range(nz):
        lat_copy(t).start()

    for load in loads[:3]:
        load.wait()
    columns = []
    for head in range(nz):
        at = slice(head * DV, (head + 1) * DV)
        first = first_s[:, at].astype(jnp.float32)
        second = second_s[:, at].astype(jnp.float32)
        mixed = first - lambda_ref[head] * second
        inverse = lax.rsqrt(jnp.mean(mixed * mixed, axis=-1, keepdims=True) + 1e-06)
        normed = mixed * inverse
        grad_out = cot_s[:, at].astype(jnp.float32)
        mean_dot = jnp.mean(grad_out * normed, axis=-1, keepdims=True)
        grad_rows = (inverse * (grad_out - normed * mean_dot)).astype(jnp.bfloat16)
        grad_s[:, at] = grad_rows
        widened = grad_rows.astype(jnp.float32)
        columns.append(jnp.sum(widened * first, axis=-1, keepdims=True))
        columns.append(jnp.sum(widened * second, axis=-1, keepdims=True))
    dots = jnp.concatenate(columns, axis=1).T
    for head in range(nz):
        pair = slice(2 * head, 2 * head + 2)
        stat_s[head] = jnp.concatenate(
            [lse_ref[pair, :], dots[pair, :], jnp.zeros((4, rows), jnp.float32)], axis=0
        )
    for k in range(1, nz):
        send(2, k).start()
        send(1, k).start()
    own_do = pltpu.make_async_copy(grad_s.at[:, lanes(z)], do_all.at[chunk(z, rows)], own_sem.at[2])
    own_do.start()
    stat_r[z] = stat_s[z]
    for k in range(1, nz):
        send(3, k).start()
    for load in loads[3:]:
        load.wait()
    v_s[...] = jnp.dot(lat_s[...], w_s[...], preferred_element_type=jnp.float32).astype(
        jnp.bfloat16
    )
    for k in range(1, nz):
        send(4, k).start()
    own_v = pltpu.make_async_copy(v_s.at[:, lanes(z)], v_all.at[chunk(sp, rows)], own_sem.at[3])
    own_v.start()
    passed(1, 0, v_s.at[:, lanes(z)], sp).start()

    for part in range(3):
        for k in range(1, nz):
            send(part, k).wait_recv()
    own_q.wait()
    own_k.wait()
    own_do.wait()
    own_v.wait()
    scale = jnp.bfloat16(DH**-0.5)
    queries = q_all[...] * scale
    half = lax.broadcasted_iota(jnp.int32, queries.shape, 1) < DH
    q0_s[...] = jnp.where(half, queries, jnp.zeros_like(queries))
    q1_s[...] = jnp.where(half, jnp.zeros_like(queries), queries)
    stats = jnp.concatenate(
        [stat_r[c] for c in range(nz)] + [jnp.full((8, tail), 1e30, jnp.float32)], axis=1
    )
    for t in range(tiles):
        stat_t[t] = stats[:, t * BLOCK : (t + 1) * BLOCK]
    weight = lambda_ref[z]

    def column(j):
        key_rows = chunk(j, rows)
        keys = k_all[key_rows, :]
        keys_t = keys.T
        dk_s[...] = jnp.zeros_like(dk_s)
        dv_s[...] = jnp.zeros_like(dv_s)
        lowest = (j + 1 - y) // 2
        begin = (lowest * rows) // BLOCK
        middle = jnp.minimum(((lowest + 1) * rows - 1) // BLOCK + 1, tiles)
        begin = jnp.where(lowest == nz, tiles, begin)

        def tile(t, masked):
            at = chunk(t, BLOCK)
            q0, q1, grads = q0_s[at, :], q1_s[at, :], do_all[at, :]
            keys = k_all[key_rows, :]
            stat = stat_t[t]
            s0 = lax.dot_general(keys, q0, NT, preferred_element_type=jnp.float32)
            s1 = lax.dot_general(keys, q1, NT, preferred_element_type=jnp.float32)
            d_attn = lax.dot_general(
                v_all[key_rows, :], grads, NT, preferred_element_type=jnp.float32
            )
            x0 = s0 - stat[0:1, :]
            x1 = s1 - stat[1:2, :]
            if masked:
                place = t * BLOCK + lax.broadcasted_iota(jnp.int32, (1, BLOCK), 1)
                shift = y * rows - j * rows + place
                for c in range(1, nz):
                    shift = shift + jnp.where(place >= c * rows, rows, 0)
                seen = lax.broadcasted_iota(jnp.int32, (rows, BLOCK), 0) <= shift
                x0 = jnp.where(seen, x0, -1e30)
                x1 = jnp.where(seen, x1, -1e30)
            p0 = jnp.exp(x0)
            p1 = weight * jnp.exp(x1)
            ds0 = (p0 * (d_attn - stat[2:3, :])).astype(jnp.bfloat16)
            ds1 = (p1 * (stat[3:4, :] - d_attn)).astype(jnp.bfloat16)
            w = (p0 - p1).astype(jnp.bfloat16)
            dk_s[...] += jnp.dot(ds0, q0, preferred_element_type=jnp.float32) + jnp.dot(
                ds1, q1, preferred_element_type=jnp.float32
            )
            dv_s[...] += jnp.dot(w, grads, preferred_element_type=jnp.float32)
            dqt_s[t, :DH, :] += jnp.dot(keys_t[:DH], ds0, preferred_element_type=jnp.float32)
            dqt_s[t, DH:, :] += jnp.dot(keys_t[DH:], ds1, preferred_element_type=jnp.float32)

        def first_tiles(t, carry):
            tile(t, True)
            return carry

        def other_tiles(t, carry):
            tile(t, False)
            return carry

        lax.fori_loop(begin, middle, first_tiles, 0)
        lax.fori_loop(jnp.maximum(begin, middle), tiles, other_tiles, 0)

    def step(i, carry):
        k, side = i // 2, i % 2
        at = level(z, k, nz)
        mine = 2 * at + y

        @pl.when(side == 0)
        def _():
            @pl.when(k > 0)
            def _():
                for part, kept in ((3, k_all), (4, v_all)):
                    remote(
                        kept.at[chunk(mine, rows)], kept.at[chunk(mine, rows)],
                        send_sem.at[part, k], recv_sem.at[part, k], {"sp": mine}
                    ).wait_recv()
                    passed(part - 3, k, kept.at[chunk(mine, rows)], mine).start()

        @pl.when(side == 1)
        def _():
            for part, kept in ((0, k_all), (1, v_all)):
                other = 2 * at + 1 - y
                passed(part, k, kept.at[chunk(other, rows)], other).wait_recv()

        column(2 * at + (y + side) % 2)

        @pl.when(side == 0)
        def _():
            dkm_ref[at] = dk_s[...]
            dvm_ref[at] = dv_s[...]

        @pl.when(side == 1)
        def _():
            dko_ref[at] = dk_s[...].astype(jnp.bfloat16)
            dvo_ref[at] = dv_s[...].astype(jnp.bfloat16)

        return carry

    lax.fori_loop(0, 2 * nz, step, 0)
    for t in range(tiles):
        dq_ref[t * BLOCK : (t + 1) * BLOCK, :] = (dqt_s[t] * DH ** (-0.5)).T.astype(jnp.bfloat16)
    for t in range(nz):
        lat_copy(t).wait_recv()
        lat_copy(t).wait_send()
    for part in range(5):
        for k in range(1, nz):
            send(part, k).wait_send()
    for part in range(2):
        for k in range(nz):
            passed(part, k, (k_all, v_all)[part].at[chunk(sp, rows)], sp).wait_send()


def forward(queries, keys, latents, value_weight, first, second, cotangent, lse, head_lambda, n):
    rows = queries.shape[0]
    depth, wide = value_weight.shape
    nz = n // 2
    width = depth // n
    tiles = pad_tiles(nz * rows)
    dense = jnp.bfloat16
    vmem = pl.BlockSpec(memory_space=pltpu.VMEM)
    hbm = pl.BlockSpec(memory_space=pl.ANY)
    sem = pltpu.SemaphoreType.DMA
    piece = (nz, rows, DV)
    return pl.pallas_call(
        functools.partial(forward_kernel, nz),
        out_shape=[
            jax.ShapeDtypeStruct((tiles * BLOCK, DV), dense),
            jax.ShapeDtypeStruct(piece, jnp.float32),
            jax.ShapeDtypeStruct(piece, jnp.float32),
            jax.ShapeDtypeStruct(piece, dense),
            jax.ShapeDtypeStruct(piece, dense),
            jax.ShapeDtypeStruct((nz, rows, width), dense),
        ],
        in_specs=[hbm] * 7 + [vmem, pl.BlockSpec(memory_space=pltpu.SMEM)],
        out_specs=[vmem] * 6,
        scratch_shapes=[
            pltpu.VMEM((rows, wide), dense),
            pltpu.VMEM((rows, wide), dense),
            pltpu.VMEM((rows, wide), dense),
            pltpu.VMEM((rows, depth), dense),
            pltpu.VMEM((depth, wide), dense),
            pltpu.VMEM((rows, wide), dense),
            pltpu.VMEM((nz, 8, rows), jnp.float32),
            pltpu.VMEM((rows, wide), dense),
            pltpu.VMEM((tiles * BLOCK, DV), dense),
            pltpu.VMEM((tiles * BLOCK, DV), dense),
            pltpu.VMEM((n * rows, DV), dense),
            pltpu.VMEM((n * rows, DV), dense),
            pltpu.VMEM((nz, 8, rows), jnp.float32),
            pltpu.VMEM((tiles * BLOCK, DV), dense),
            pltpu.VMEM((tiles * BLOCK, DV), dense),
            pltpu.VMEM((tiles, 8, BLOCK), jnp.float32),
            pltpu.VMEM((tiles, 2 * DH, BLOCK), jnp.float32),
            pltpu.VMEM((rows, DV), jnp.float32),
            pltpu.VMEM((rows, DV), jnp.float32),
            sem((5,)),
            sem((4,)),
            sem((5, nz)),
            sem((5, nz)),
            sem((2, nz)),
            sem((2, nz)),
            sem((nz,)),
            sem((nz,)),
        ],
        compiler_params=pltpu.CompilerParams(collective_id=1, has_side_effects=True),
    )(queries, keys, latents, value_weight, first, second, cotangent, lse, head_lambda)


def back_kernel(
    nz, ntp, dq_ref, dkm_ref, dvm_ref, dko_ref, dvo_ref, latp_ref, lat_ref, w_ref,
    q_home, k_home, gl_ref, gw_ref,
    lat_s, w_s, dky_s, dvy_s, dks_s, dvs_s, v_pair, gl_send, gl_recv,
    up_send, up_recv, down_send, down_recv, sum_s,
    load_sem, own_sem, q_send, q_recv, y_send, y_recv, z_send, z_recv, h_send, h_recv,
    t_send, t_recv, u_send, u_recv, d_send, d_recv
):
    sp, tp = lax.axis_index("sp"), lax.axis_index("tp")
    z, y = sp // 2, lax.rem(sp, 2)
    rows = dkm_ref.shape[1]
    width = latp_ref.shape[2]
    parts = up_send.shape[1]
    piece = width // parts
    partner = {"sp": 2 * z + 1 - y}
    peers = [{"sp": 2 * level(z, k, nz) + y} for k in range(1, nz)]
    sides = [{"tp": lax.rem(tp + step, ntp)} for step in range(1, ntp)]
    lat_load = pltpu.make_async_copy(lat_ref, lat_s, load_sem.at[0])
    w_load = pltpu.make_async_copy(w_ref, w_s, load_sem.at[1])
    lat_load.start()
    w_load.start()
    arrived = greet(peers + [partner] + sides)
    own_q = pltpu.make_async_copy(
        dq_ref.at[chunk(z, rows)], q_home.at[:, lanes(z)], own_sem.at[0]
    )
    own_q.start()
    arrived()

    def q_copy(k):
        at = level(z, k, nz)
        return remote(
            dq_ref.at[chunk(at, rows)], q_home.at[:, lanes(z)],
            q_send.at[k], q_recv.at[k], peers[k - 1]
        )

    def y_copy(part, k):
        at = level(z, k, nz)
        src, dst = ((dvo_ref, dvy_s), (dko_ref, dky_s))[part]
        return remote(src.at[at], dst.at[at], y_send.at[part, k], y_recv.at[part, k], partner)

    def z_copy(part, k):
        at = level(z, k, nz)
        src = (dvs_s, dks_s)[part].at[at]
        dst = v_pair.at[0:rows, lanes(z)] if part == 0 else k_home.at[:, lanes(z)]
        return remote(src, dst, z_send.at[part, k], z_recv.at[part, k], peers[k - 1])

    def home_copy(k):
        head = level(z, k, nz)
        return remote(
            v_pair.at[0:rows, lanes(head)], v_pair.at[rows : 2 * rows, lanes(head)],
            h_send.at[k], h_recv.at[k], partner
        )

    order = list(range(1, nz)) + [0]
    for part in range(2):
        for k in order:
            y_copy(part, k).start()
    for k in range(1, nz):
        q_copy(k).start()
    for part, (mine, got, total) in enumerate(
        ((dvm_ref, dvy_s, dvs_s), (dkm_ref, dky_s, dks_s))
    ):
        for k in order:
            at = level(z, k, nz)
            y_copy(part, k).wait_recv()
            added = (mine[at] + got[at].astype(jnp.float32)).astype(jnp.bfloat16)
            if k == 0:
                if part == 0:
                    v_pair[0:rows, lanes(z)] = added
                else:
                    k_home[:, lanes(z)] = added
            else:
                total[at] = added
                z_copy(part, k).start()
    home_copy(0).start()
    for k in range(1, nz):
        z_copy(0, k).wait_recv()
        home_copy(k).start()

    w_load.wait()
    own_rows = v_pair[0:rows, :]
    wide = gl_ref.shape[1]

    def t_copy(step):
        return remote(
            gl_send.at[step], gl_recv.at[step], t_send.at[step], t_recv.at[step], sides[step - 1]
        )

    def latent_term(at):
        return lax.dot_general(
            own_rows, w_s[chunk(at, wide), :], NT, preferred_element_type=jnp.float32
        ).astype(jnp.bfloat16)

    for step in range(1, ntp):
        gl_send[step] = latent_term(lax.rem(tp + step, ntp))
        t_copy(step).start()
    gl_send[0] = latent_term(tp)
    lat_load.wait()
    for k in range(nz):
        home_copy(k).wait_recv()

    def term(t, s):
        at = pl.ds(pl.multiple_of((2 * t + y) * width + s * piece, piece), piece)
        own = lat_s[:, at]
        other = latp_ref[t, :, s * piece : (s + 1) * piece]
        return lax.dot_general(
            jnp.concatenate([own, other], axis=0), v_pair[...], TN,
            preferred_element_type=jnp.float32,
        )

    def line_copy(up, t, s):
        if up:
            return remote(
                up_send.at[t, s], up_recv.at[t, s], u_send.at[t, s], u_recv.at[t, s],
                {"sp": 2 * (z + 1) + y}
            )
        return remote(
            down_send.at[t, s], down_recv.at[t, s], d_send.at[t, s], d_recv.at[t, s],
            {"sp": 2 * (z - 1) + y}
        )

    hops = []
    for i in range(nz - 1):
        hops += [(True, nz - 1 - i), (False, i)]

    for up, t in hops:
        for s in range(parts):
            @pl.when((z < t) if up else (z > t))
            def _():
                sum_s[...] = term(t, s)

                @pl.when((z > 0) if up else (z < nz - 1))
                def _():
                    line_copy(up, t, s).wait_recv()
                    sum_s[...] += (up_recv if up else down_recv)[t, s].astype(jnp.float32)

                (up_send if up else down_send)[t, s] = sum_s[...].astype(jnp.bfloat16)
                line_copy(up, t, s).start()

    own_q.wait()
    total = gl_send[0].astype(jnp.float32)
    for step in range(1, ntp):
        t_copy(step).wait_recv()
        total = total + gl_recv[step].astype(jnp.float32)
    gl_ref[...] = total.astype(jnp.bfloat16)
    for s in range(parts):
        at = slice(s * piece, (s + 1) * piece)
        own = pl.ds(pl.multiple_of((2 * z + y) * width + s * piece, piece), piece)
        gw_ref[at, :] = lax.dot_general(
            jnp.concatenate([lat_s[:, own], latp_ref[z, :, at]], axis=0), v_pair[...], TN,
            preferred_element_type=jnp.float32,
        )
    for k in range(1, nz):
        q_copy(k).wait_recv()
        z_copy(1, k).wait_recv()
    for t in range(nz):
        for s in range(parts):
            at = slice(s * piece, (s + 1) * piece)
            if t > 0:
                @pl.when(z == t)
                def _():
                    line_copy(True, t, s).wait_recv()
                    gw_ref[at, :] += up_recv[t, s].astype(jnp.float32)
            if t < nz - 1:
                @pl.when(z == t)
                def _():
                    line_copy(False, t, s).wait_recv()
                    gw_ref[at, :] += down_recv[t, s].astype(jnp.float32)
    for up, t in hops:
        for s in range(parts):
            @pl.when((z < t) if up else (z > t))
            def _():
                line_copy(up, t, s).wait_send()
    for k in range(1, nz):
        q_copy(k).wait_send()
        for part in range(2):
            z_copy(part, k).wait_send()
    for k in range(nz):
        home_copy(k).wait_send()
        for part in range(2):
            y_copy(part, k).wait_send()
    for step in range(1, ntp):
        t_copy(step).wait_send()


def back(dq, dkm, dvm, dko, dvo, latp, latents, value_weight, ntp):
    nz, rows, _ = dkm.shape
    depth, wide = value_weight.shape
    width = latp.shape[2]
    parts = 2 if width % 256 == 0 else 1
    dense = jnp.bfloat16
    vmem = pl.BlockSpec(memory_space=pltpu.VMEM)
    hbm = pl.BlockSpec(memory_space=pl.ANY)
    sem = pltpu.SemaphoreType.DMA
    share = depth // ntp
    line = pltpu.VMEM((nz, parts, width // parts, wide), dense)
    return pl.pallas_call(
        functools.partial(back_kernel, nz, ntp),
        out_shape=[
            jax.ShapeDtypeStruct((rows, wide), dense),
            jax.ShapeDtypeStruct((rows, wide), dense),
            jax.ShapeDtypeStruct((rows, share), dense),
            jax.ShapeDtypeStruct((width, wide), jnp.float32),
        ],
        in_specs=[vmem] * 6 + [hbm] * 2,
        out_specs=[vmem] * 4,
        scratch_shapes=[
            pltpu.VMEM((rows, depth), dense),
            pltpu.VMEM((depth, wide), dense),
        ]
        + [pltpu.VMEM((nz, rows, DV), dense)] * 4
        + [
            pltpu.VMEM((2 * rows, wide), dense),
            pltpu.VMEM((ntp, rows, share), dense),
            pltpu.VMEM((ntp, rows, share), dense),
        ]
        + [line] * 4
        + [
            pltpu.VMEM((width // parts, wide), jnp.float32),
            sem((2,)),
            sem((1,)),
            sem((nz,)),
            sem((nz,)),
            sem((2, nz)),
            sem((2, nz)),
            sem((2, nz)),
            sem((2, nz)),
            sem((nz,)),
            sem((nz,)),
            sem((ntp,)),
            sem((ntp,)),
            sem((nz, parts)),
            sem((nz, parts)),
            sem((nz, parts)),
            sem((nz, parts)),
        ],
        compiler_params=pltpu.CompilerParams(collective_id=2, has_side_effects=True),
    )(dq, dkm, dvm, dko, dvo, latp, latents, value_weight)


def finish_kernel(q_ref, k_ref, gl_ref, gw_ref, q_out, k_out, gl_out, gw_out):
    q_out[...] = q_ref[...].astype(jnp.float32)
    k_out[...] = k_ref[...].astype(jnp.float32)
    gl_out[...] = gl_ref[...]
    gw_out[...] = gw_ref[...]


def finish(q_home, k_home, gl, gw):
    vmem = pl.BlockSpec(memory_space=pltpu.VMEM)
    kinds = ((q_home, jnp.float32), (k_home, jnp.float32), (gl, gl.dtype), (gw, gw.dtype))
    return pl.pallas_call(
        finish_kernel,
        out_shape=[jax.ShapeDtypeStruct(a.shape, kind) for a, kind in kinds],
        in_specs=[vmem] * 4,
        out_specs=[vmem] * 4,
    )(q_home, k_home, gl, gw)


def by_level(
    queries, key_vectors, latents, value_weight, log_sums, out_first, out_second, cotangent,
    head_lambda
):
    n, ntp = lax.axis_size("sp"), lax.axis_size("tp")
    *grads, latp = forward(
        queries, key_vectors, latents, value_weight, out_first, out_second, cotangent,
        log_sums.T, head_lambda, n
    )
    return tuple(finish(*back(*grads, latp, latents, value_weight, ntp)))


def dispatch(queries, key_vectors, latents, value_weight, log_sums, *rest):
    n, ntp = lax.axis_size("sp"), lax.axis_size("tp")
    rows, depth = latents.shape
    heads = rest[-1].shape[0]
    fits = heads * 2 == n and heads & (heads - 1) == 0 and heads > 1
    fits = fits and rows % 32 == 0 and BLOCK <= rows
    fits = fits and depth % (n * DV) == 0 and depth % (ntp * DV) == 0
    fits = fits and depth // ntp == value_weight.shape[1]
    run = by_level if fits else per_device
    return run(queries, key_vectors, latents, value_weight, log_sums, *rest)


def solution(mesh):
    return jax.shard_map(
        dispatch,
        mesh=mesh,
        in_specs=(
            P("sp", "tp"),
            P("sp", "tp"),
            P("sp", None),
            P(None, "tp"),
            P("sp", "tp"),
            P("sp", "tp"),
            P("sp", "tp"),
            P("sp", "tp"),
            P("tp"),
        ),
        out_specs=(P("sp", "tp"), P("sp", "tp"), P("sp", "tp"), P("sp", "tp")),
        check_vma=False,
    )
```

time: 164 us -> 104 us (0.63)
  Pallas kernels: 139 us -> 103 us
  between operations: 14.1 us -> 0.65 us
  matrix products: 5.54 us -> 0 us
  local copies, waits for them, and re-layouts: 5.11 us -> 0 us
    pallas_call x5 -> x3, Pallas kernels: 139 us -> 103 us  [the longest x1 50.7 us: forward(): pl.pallas_call(functools.partial(forward_kernel, nz), out_shape=[jax.Shap...]
    dot_general x2 -> x0, matrix products: 5.54 us -> none  [the longest x1 2.79 us: by_unit(): lax.dot_general(values_grad, value_weight, (((1,), (1,)), ((), ())), pref...]
    unnamed x3 -> x0, local copies, waits for them, and re-layouts: 3.41 us -> none
  transfers between devices with their start and end apart: 1 -> 0, of which waited for: 0 -> 0; matrix products, arithmetic and copies ran while one was open for 0% -> 0% of each run, Pallas kernels for 23% -> 0%
where the time goes in v1:
time: 104 us; the launch traced here: 103 us
  Pallas kernels  103 us (99%)
    pallas_call x1, Pallas kernels, forward(): pl.pallas_call(functools.partial(forward_kernel, nz), out_shape=[jax.Shap...  50.7 us
    pallas_call x1, Pallas kernels, back(): pl.pallas_call(functools.partial(back_kernel, nz, ntp), out_shape=[jax.Sh...  49.3 us
    pallas_call x1, Pallas kernels, finish(): pl.pallas_call(finish_kernel, out_shape=[jax.ShapeDtypeStruct(a.shape, ki...  2.63 us

profile of v1, /device:TPU:0, one launch (start us, length us, event | category | flops | bytes accessed | tf_op | source)
XLA Modules:
  0.0 103.3 jit_solution(15803436812457079492)
XLA Ops:
  0.6 50.7 %shard_map.120 = (bf16[1280,128]{1,0:T(8,128)(2,1)}, f32[4,288,128]{2,1,0:T(8,128)}, f32[4,288,128]{2,1,0:T(8,128)}, bf16[4,288,128]{2,1,0:T(8,128)(2,1)}, bf16[...) custom-call(bf16[288,512]{1,0:T(8,128)(2,1)} %q_ref.1, bf16[288,512]{1,0:T(8,128)(2,1)} %k_ref.1, ...), custom_call_target="tpu_custom_call" | custom-call | tf_op jit(solution)/shard_map/pallas_call | solution.py:442
  51.4 49.3 %shard_map.121 = (bf16[288,512]{1,0:T(8,128)(2,1)}, bf16[288,512]{1,0:T(8,128)(2,1)}, bf16[288,512]{1,0:T(8,128)(2,1)}, f32[256,512]{1,0:T(8,128)}) custom-call(bf16[1280,128]{1,0:T(8,128)(2,1)} %get-tuple-element.14.dq_ref, f32[4,288,128]{2,1,0:T(8,128)} %get-tuple-element.15.dkm_ref, f32[4,288,128]{2,1,0:T(8,128)} %get-tuple-element.16.dvm_ref, ...), custom_call_target="tpu_custom_call" | custom-call | tf_op jit(solution)/shard_map/pallas_call | solution.py:683
  100.7 2.6 %shard_map.122 = (f32[288,512]{1,0:T(8,128)}, f32[288,512]{1,0:T(8,128)}, bf16[288,512]{1,0:T(8,128)(2,1)}, f32[256,512]{1,0:T(8,128)}) custom-call(bf16[288,512]{1,0:T(8,128)(2,1)} %get-tuple-element.20.q_ref, bf16[288,512]{1,0:T(8,128)(2,1)} %get-tuple-element.21.k_ref, bf16[288,512]{1,0:T(8,128)(2,1)} %get-tuple-element.22.gl_ref, ...), custom_call_target="tpu_custom_call" | custom-call | tf_op jit(solution)/shard_map/pallas_call | solution.py:737

commit v2 on v1

v2 whole, which is shorter than its diff:
```python
import functools

import jax
import jax.numpy as jnp
from jax import lax
from jax.experimental import pallas as pl
from jax.experimental.pallas import tpu as pltpu
from jax.sharding import PartitionSpec as P

DH = 64
DV = 128
BLOCK = 256


def row_terms(out_first, out_second, cotangent, head_lambda):
    count = out_first.shape[0]
    head_count = head_lambda.shape[0]
    first = out_first.astype(jnp.float32).reshape(count, head_count, DV)
    second = out_second.astype(jnp.float32).reshape(count, head_count, DV)
    mixed = first - head_lambda[None, :, None] * second
    inverse = lax.rsqrt(jnp.mean(mixed * mixed, axis=-1, keepdims=True) + 1e-06)
    normed = mixed * inverse
    grad_out = cotangent.astype(jnp.float32).reshape(count, head_count, DV)
    grad_mixed = inverse * (grad_out - normed * jnp.mean(grad_out * normed, axis=-1, keepdims=True))
    grad_rows = grad_mixed.astype(jnp.bfloat16)
    widened = lax.optimization_barrier(grad_rows).astype(jnp.float32)
    row_dots = jnp.stack(
        [jnp.sum(widened * first, axis=-1), jnp.sum(widened * second, axis=-1)], axis=-1
    )
    return (grad_rows.reshape(count, head_count * DV), row_dots.reshape(count, head_count * 2))


def block_grads(
    query_rows, grad_rows, lse_rows, dot_rows, query_pos, key_rows, value_rows, key_pos, head_lambda
):
    count = query_rows.shape[0]
    width = key_rows.shape[0]
    head_count = head_lambda.shape[0]
    score_scale = DH ** (-0.5)
    query_heads = query_rows.reshape(count, head_count, 2, DH)
    key_heads = key_rows.reshape(width, head_count, 2, DH)
    grad_heads = grad_rows.reshape(count, head_count, DV)
    value_heads = value_rows.reshape(width, head_count, DV)
    scores = (
        jnp.einsum("nhad,mhad->hanm", query_heads, key_heads, preferred_element_type=jnp.float32)
        * score_scale
    )
    causal = query_pos[:, None] >= key_pos[None, :]
    shifts = lse_rows.reshape(count, head_count, 2).transpose(1, 2, 0)[..., None]
    probs = jnp.exp(jnp.where(causal, scores - shifts, -1e30))
    d_attn = jnp.einsum("nhe,mhe->hnm", grad_heads, value_heads, preferred_element_type=jnp.float32)
    dots = dot_rows.reshape(count, head_count, 2).transpose(1, 2, 0)[..., None]
    map_weight = jnp.stack([jnp.ones_like(head_lambda), -head_lambda], axis=1)[:, :, None, None]
    d_scores = (map_weight * probs * (d_attn[:, None] - dots)).astype(jnp.bfloat16)
    weights = (probs[:, 0] - head_lambda[:, None, None] * probs[:, 1]).astype(jnp.bfloat16)
    grad_q = (
        jnp.einsum("hanm,mhad->nhad", d_scores, key_heads, preferred_element_type=jnp.float32)
        * score_scale
    )
    grad_k = (
        jnp.einsum("hanm,nhad->mhad", d_scores, query_heads, preferred_element_type=jnp.float32)
        * score_scale
    )
    grad_v = jnp.einsum("hnm,nhe->mhe", weights, grad_heads, preferred_element_type=jnp.float32)
    return (grad_q.reshape(count, -1), grad_k.reshape(width, -1), grad_v.reshape(width, -1))


def per_device(
    queries,
    key_vectors,
    latents,
    value_weight,
    log_sums,
    out_first,
    out_second,
    cotangent,
    head_lambda,
):
    local_rows = queries.shape[0]
    offset = lax.axis_index("sp") * local_rows
    positions = offset + jnp.arange(local_rows, dtype=jnp.int32)
    last_row = offset + local_rows - 1
    values = jnp.dot(latents, value_weight, preferred_element_type=jnp.float32).astype(jnp.bfloat16)
    grad_rows, row_dots = row_terms(out_first, out_second, cotangent, head_lambda)
    gathered_stats = (
        lax.all_gather(log_sums, "sp", axis=0, tiled=True),
        lax.all_gather(row_dots, "sp", axis=0, tiled=True),
    )
    key_rows = lax.all_gather(key_vectors, "sp", axis=0, tiled=True)
    value_rows = lax.all_gather(values, "sp", axis=0, tiled=True)
    count = key_rows.shape[0]

    def compute(current):
        key_pos = jnp.arange(count, dtype=jnp.int32)
        grad_q, unused_k, unused_v = block_grads(
            queries,
            grad_rows,
            log_sums,
            row_dots,
            positions,
            key_rows,
            value_rows,
            key_pos,
            head_lambda,
        )
        return grad_q

    grad_queries = lax.cond(
        jnp.int32(0) <= last_row,
        compute,
        lambda current: current,
        jnp.zeros((local_rows, queries.shape[1]), jnp.float32),
    )
    start_totals = (
        jnp.zeros((local_rows, key_vectors.shape[1]), jnp.float32),
        jnp.zeros((local_rows, values.shape[1]), jnp.float32),
    )
    query_rows = lax.all_gather(queries, "sp", axis=0, tiled=True)
    grad_piece = lax.all_gather(grad_rows, "sp", axis=0, tiled=True)
    add_count = query_rows.shape[0]

    def compute(current):
        query_pos = jnp.arange(add_count, dtype=jnp.int32)
        lse_rows = gathered_stats[0]
        dot_rows = gathered_stats[1]
        unused_q, grad_k, grad_v = block_grads(
            query_rows,
            grad_piece,
            lse_rows,
            dot_rows,
            query_pos,
            key_vectors,
            values,
            positions,
            head_lambda,
        )
        return (grad_k, grad_v)

    grad_keys, grad_values = lax.cond(
        jnp.int32(0) + add_count - 1 >= offset, compute, lambda current: current, start_totals
    )
    values_grad = grad_values.astype(jnp.bfloat16)
    grad_weight = lax.psum_scatter(
        lax.dot_general(
            latents, values_grad, (((0,), (0,)), ((), ())), preferred_element_type=jnp.float32
        ).astype(jnp.bfloat16),
        "sp",
        scatter_dimension=0,
        tiled=True,
    ).astype(jnp.float32)
    latent_partial = lax.dot_general(
        values_grad, value_weight, (((1,), (1,)), ((), ())), preferred_element_type=jnp.float32
    )
    grad_latents = lax.psum_scatter(
        latent_partial.astype(jnp.bfloat16), "tp", scatter_dimension=1, tiled=True
    )
    return (grad_queries, grad_keys, grad_latents, grad_weight)


def level(z, k, nz):
    bit, out = 1, z
    while bit < nz:
        out = out + ((k // bit) % 2) * bit * (1 - 2 * ((z // bit) % 2))
        bit *= 2
    return out


def lanes(index, width=DV):
    return pl.ds(pl.multiple_of(index * width, width), width)


def chunk(index, rows):
    return pl.ds(pl.multiple_of(index * rows, rows), rows)


def remote(src, dst, send_sem, recv_sem, where):
    return pltpu.make_async_remote_copy(
        src_ref=src,
        dst_ref=dst,
        send_sem=send_sem,
        recv_sem=recv_sem,
        device_id=where,
        device_id_type=pl.DeviceIdType.MESH,
    )


def greet(devices):
    barrier = pltpu.get_barrier_semaphore()
    for device in devices:
        pl.semaphore_signal(
            barrier, inc=1, device_id=device, device_id_type=pl.DeviceIdType.MESH
        )
    return lambda: pl.semaphore_wait(barrier, len(devices))


NT = (((1,), (1,)), ((), ()))
TN = (((0,), (0,)), ((), ()))


def level_kernel(
    nz, ntp, q_ref, k_ref, lat_ref, w_ref, first_ref, second_ref, cot_ref, lse_ref, lambda_ref,
    q_home, k_home, gl_ref, gw_ref,
    first_s, second_s, cot_s, lat_s, w_s, grad_s, stat_s, v_s, q_all, do_all, k_all, v_all,
    stat_r, k0_s, k1_s, latp_s, qq_s, wide_s, dq_acc, dq_s, dkt_s, dvt_s, dk_s, dv_s,
    dko_s, dvo_s, dky_s, dvy_s, dks_s, dvs_s, v_pair, gl_s, gl_recv,
    up_send, up_recv, down_send, down_recv, sum_s,
    load_sem, own_sem, send_sem, recv_sem, pass_send, pass_recv, lat_send, lat_recv,
    q_send, q_recv, y_send, y_recv, z_send, z_recv, h_send, h_recv, t_send, t_recv,
    u_send, u_recv, d_send, d_recv
):
    sp, tp = lax.axis_index("sp"), lax.axis_index("tp")
    z, y = sp // 2, lax.rem(sp, 2)
    rows = q_ref.shape[0]
    width = latp_s.shape[2]
    partner = {"sp": 2 * z + 1 - y}
    peers = [{"sp": 2 * level(z, k, nz) + y} for k in range(1, nz)]
    bits = [1 << b for b in range(ntp.bit_length() - 1)]
    sides = {bit: {"tp": level(tp, bit, ntp)} for bit in bits}
    loads = [
        pltpu.make_async_copy(src, dst, load_sem.at[i])
        for i, (src, dst) in enumerate(
            [(lat_ref, lat_s), (w_ref, w_s), (first_ref, first_s), (second_ref, second_s),
             (cot_ref, cot_s)]
        )
    ]
    for load in loads:
        load.start()
    arrived = greet(peers + [partner] + list(sides.values()))
    own_q = pltpu.make_async_copy(q_ref.at[:, lanes(z)], q_all.at[z], own_sem.at[0])
    own_k = pltpu.make_async_copy(k_ref.at[:, lanes(z)], k_all.at[chunk(sp, rows)], own_sem.at[1])
    own_q.start()
    own_k.start()
    dkt_s[...] = jnp.zeros_like(dkt_s)
    dvt_s[...] = jnp.zeros_like(dvt_s)
    arrived()

    def send(part, k):
        to = level(z, k, nz)
        src, dst = {
            0: (q_ref.at[:, lanes(to)], q_all.at[z]),
            1: (grad_s.at[:, lanes(to)], do_all.at[z]),
            2: (stat_s.at[to], stat_r.at[z]),
            3: (k_ref.at[:, lanes(to)], k_all.at[chunk(sp, rows)]),
            4: (v_s.at[:, lanes(to)], v_all.at[chunk(sp, rows)]),
        }[part]
        return remote(src, dst, send_sem.at[part, k], recv_sem.at[part, k], peers[k - 1])

    def passed(part, k, own=None):
        kept = (k_all, v_all)[part]
        at = chunk(2 * level(z, k, nz) + y, rows)
        src = kept.at[at] if own is None else own
        return remote(src, kept.at[at], pass_send.at[part, k], pass_recv.at[part, k], partner)

    def lat_copy(t):
        return remote(
            lat_ref.at[:, lanes(2 * t + 1 - y, width)], latp_s.at[t],
            lat_send.at[t], lat_recv.at[t], partner
        )

    for k in range(1, nz):
        send(3, k).start()
    passed(0, 0, k_ref.at[:, lanes(z)]).start()
    for load in loads[:2]:
        load.wait()
    v_s[...] = jnp.dot(lat_s[...], w_s[...], preferred_element_type=jnp.float32).astype(
        jnp.bfloat16
    )
    for k in range(1, nz):
        send(4, k).start()
    passed(1, 0, v_s.at[:, lanes(z)]).start()
    own_v = pltpu.make_async_copy(v_s.at[:, lanes(z)], v_all.at[chunk(sp, rows)], own_sem.at[2])
    own_v.start()
    for load in loads[2:]:
        load.wait()
    columns = []
    for head in range(nz):
        at = slice(head * DV, (head + 1) * DV)
        first = first_s[:, at].astype(jnp.float32)
        second = second_s[:, at].astype(jnp.float32)
        mixed = first - lambda_ref[head] * second
        inverse = lax.rsqrt(jnp.mean(mixed * mixed, axis=-1, keepdims=True) + 1e-06)
        normed = mixed * inverse
        grad_out = cot_s[:, at].astype(jnp.float32)
        mean_dot = jnp.mean(grad_out * normed, axis=-1, keepdims=True)
        grad_rows = (inverse * (grad_out - normed * mean_dot)).astype(jnp.bfloat16)
        grad_s[:, at] = grad_rows
        widened = grad_rows.astype(jnp.float32)
        columns.append(jnp.sum(widened * first, axis=-1, keepdims=True))
        columns.append(jnp.sum(widened * second, axis=-1, keepdims=True))
    dots = jnp.concatenate(columns, axis=1).T
    for head in range(nz):
        pair = slice(2 * head, 2 * head + 2)
        stat_s[head] = jnp.concatenate(
            [lse_ref[pair, :], dots[pair, :], jnp.zeros((4, rows), jnp.float32)], axis=0
        )
    for k in range(1, nz):
        for part in (2, 0, 1):
            send(part, k).start()
    own_do = pltpu.make_async_copy(grad_s.at[:, lanes(z)], do_all.at[z], own_sem.at[3])
    own_do.start()
    stat_r[z] = stat_s[z]

    for part in (3, 4):
        for k in range(1, nz):
            send(part, k).wait_recv()
            passed(part - 3, k).start()
    for t in range(nz):
        lat_copy(t).start()
    own_k.wait()
    own_v.wait()
    for part in range(2):
        for k in range(nz):
            passed(part, k).wait_recv()
    keys = k_all[...]
    half = lax.broadcasted_iota(jnp.int32, keys.shape, 1) < DH
    k0_s[...] = jnp.where(half, keys, jnp.zeros_like(keys))
    k1_s[...] = jnp.where(half, jnp.zeros_like(keys), keys)
    weight = lambda_ref[z]
    scale = jnp.bfloat16(DH**-0.5)

    def q_copy(k):
        return remote(
            dq_s.at[k], q_home.at[:, lanes(z)], q_send.at[k], q_recv.at[k], peers[k - 1]
        )

    for k in range(nz):
        at = level(z, k, nz)
        if k == 0:
            own_q.wait()
            own_do.wait()
        else:
            for part in range(3):
                send(part, k).wait_recv()
        queries = q_all[at] * scale
        left = lax.broadcasted_iota(jnp.int32, queries.shape, 1) < DH
        qq_s[0:rows, :] = jnp.where(left, queries, jnp.zeros_like(queries))
        qq_s[rows:, :] = jnp.where(left, jnp.zeros_like(queries), queries)
        queries_t = queries.T
        grads_t = do_all[at].T
        stats = stat_r[at].T
        for i in range(4):
            wide_s[i] = jnp.broadcast_to(stats[:, i : i + 1], (rows, BLOCK))
        dq_acc[...] = jnp.zeros_like(dq_acc)
        place = 2 * at + y
        full = (place * rows + 1) // BLOCK
        end = ((place + 1) * rows - 1) // BLOCK + 1

        def tile(t, masked):
            key_rows = chunk(t, BLOCK)
            s01 = lax.dot_general(
                qq_s[...], k_all[key_rows, :], NT, preferred_element_type=jnp.float32
            )
            d_attn = lax.dot_general(
                do_all[at], v_all[key_rows, :], NT, preferred_element_type=jnp.float32
            )
            x0 = s01[:rows] - wide_s[0]
            x1 = s01[rows:] - wide_s[1]
            if masked:
                key_at = lax.broadcasted_iota(jnp.int32, (rows, BLOCK), 1) + t * BLOCK
                query_at = lax.broadcasted_iota(jnp.int32, (rows, BLOCK), 0) + place * rows
                x0 = jnp.where(key_at <= query_at, x0, -1e30)
                x1 = jnp.where(key_at <= query_at, x1, -1e30)
            p0 = jnp.exp(x0)
            p1 = weight * jnp.exp(x1)
            ds0 = (p0 * (d_attn - wide_s[2])).astype(jnp.bfloat16)
            ds1 = (p1 * (wide_s[3] - d_attn)).astype(jnp.bfloat16)
            w = (p0 - p1).astype(jnp.bfloat16)
            dq_acc[...] += jnp.dot(
                ds0, k0_s[key_rows, :], preferred_element_type=jnp.float32
            ) + jnp.dot(ds1, k1_s[key_rows, :], preferred_element_type=jnp.float32)
            columns = lanes(t, BLOCK)
            dkt_s[:DH, columns] += jnp.dot(
                queries_t[:DH], ds0, preferred_element_type=jnp.float32
            )
            dkt_s[DH:, columns] += jnp.dot(
                queries_t[DH:], ds1, preferred_element_type=jnp.float32
            )
            dvt_s[:, columns] += jnp.dot(grads_t, w, preferred_element_type=jnp.float32)

        def full_tiles(t, carry):
            tile(t, False)
            return carry

        def edge_tiles(t, carry):
            tile(t, True)
            return carry

        lax.fori_loop(0, full, full_tiles, 0)
        lax.fori_loop(full, end, edge_tiles, 0)
        grad_q = (dq_acc[...] * DH ** (-0.5)).astype(jnp.bfloat16)
        if k == 0:
            q_home[:, lanes(z)] = grad_q
        else:
            dq_s[k] = grad_q
            q_copy(k).start()

    def y_copy(part, k):
        at = level(z, k, nz)
        src, dst = ((dvo_s, dvy_s), (dko_s, dky_s))[part]
        return remote(src.at[at], dst.at[at], y_send.at[part, k], y_recv.at[part, k], partner)

    def z_copy(part, k):
        at = level(z, k, nz)
        src = (dvs_s, dks_s)[part].at[at]
        dst = v_pair.at[0:rows, lanes(z)] if part == 0 else k_home.at[:, lanes(z)]
        return remote(src, dst, z_send.at[part, k], z_recv.at[part, k], peers[k - 1])

    def home_copy(k):
        head = level(z, k, nz)
        return remote(
            v_pair.at[0:rows, lanes(head)], v_pair.at[rows : 2 * rows, lanes(head)],
            h_send.at[k], h_recv.at[k], partner
        )

    order = list(range(1, nz)) + [0]
    for part, (turned, flat, other) in enumerate(((dvt_s, dv_s, dvo_s), (dkt_s, dk_s, dko_s))):
        for t in range(flat.shape[0] // BLOCK):
            at = slice(t * BLOCK, (t + 1) * BLOCK)
            flat[at, :] = turned[:, at].T
        for k in order:
            at = level(z, k, nz)
            other[at] = flat[chunk(2 * at + 1 - y, rows), :].astype(jnp.bfloat16)
            y_copy(part, k).start()
    for part, (flat, got, total) in enumerate(((dv_s, dvy_s, dvs_s), (dk_s, dky_s, dks_s))):
        for k in order:
            at = level(z, k, nz)
            y_copy(part, k).wait_recv()
            added = flat[chunk(2 * at + y, rows), :] + got[at].astype(jnp.float32)
            added = added.astype(jnp.bfloat16)
            if k == 0:
                if part == 0:
                    v_pair[0:rows, lanes(z)] = added
                else:
                    k_home[:, lanes(z)] = added
            else:
                total[at] = added
                z_copy(part, k).start()
    home_copy(0).start()
    for k in range(1, nz):
        z_copy(0, k).wait_recv()
        home_copy(k).start()

    own_rows = v_pair[0:rows, :]
    share = gl_ref.shape[1]

    def latent_term(o):
        at = chunk(level(tp, o, ntp), share)
        return lax.dot_general(
            own_rows, w_s[at, :], NT, preferred_element_type=jnp.float32
        ).astype(jnp.bfloat16)

    def side_copy(bit, o):
        return remote(
            gl_s.at[o], gl_recv.at[o], t_send.at[o], t_recv.at[o], sides[bit]
        )

    alive = list(range(ntp))
    moves = []
    for bit in bits:
        leaving = [o for o in alive if o & bit]
        if bit == 1:
            for o in leaving:
                gl_s[o] = latent_term(o)
                side_copy(bit, o).start()
            alive = [o for o in alive if not o & bit]
            for o in alive:
                gl_s[o] = latent_term(o)
        else:
            for o in leaving:
                side_copy(bit, o).start()
            alive = [o for o in alive if not o & bit]
        moves.append((bit, leaving, alive))
        if bit != bits[-1]:
            for o in leaving:
                side_copy(bit, o).wait_recv()
            for o in alive:
                gl_s[o] = (
                    gl_s[o].astype(jnp.float32) + gl_recv[o + bit].astype(jnp.float32)
                ).astype(jnp.bfloat16)
    for t in range(nz):
        lat_copy(t).wait_recv()
    for k in range(nz):
        home_copy(k).wait_recv()

    parts = up_send.shape[1]
    piece = width // parts

    def term(t, s):
        at = pl.ds(pl.multiple_of((2 * t + y) * width + s * piece, piece), piece)
        own = lat_s[:, at]
        other = latp_s[t, :, s * piece : (s + 1) * piece]
        return lax.dot_general(
            jnp.concatenate([own, other], axis=0), v_pair[...], TN,
            preferred_element_type=jnp.float32,
        )

    def line_copy(up, t, s):
        if up:
            return remote(
                up_send.at[t, s], up_recv.at[t, s], u_send.at[t, s], u_recv.at[t, s],
                {"sp": 2 * (z + 1) + y}
            )
        return remote(
            down_send.at[t, s], down_recv.at[t, s], d_send.at[t, s], d_recv.at[t, s],
            {"sp": 2 * (z - 1) + y}
        )

    hops = []
    for i in range(nz - 1):
        hops += [(True, nz - 1 - i), (False, i)]

    for up, t in hops:
        for s in range(parts):
            @pl.when((z < t) if up else (z > t))
            def _():
                sum_s[...] = term(t, s)

                @pl.when((z > 0) if up else (z < nz - 1))
                def _():
                    line_copy(up, t, s).wait_recv()
                    sum_s[...] += (up_recv if up else down_recv)[t, s].astype(jnp.float32)

                (up_send if up else down_send)[t, s] = sum_s[...].astype(jnp.bfloat16)
                line_copy(up, t, s).start()

    last = bits[-1]
    side_copy(last, last).wait_recv()
    gl_ref[...] = (gl_s[0].astype(jnp.float32) + gl_recv[last].astype(jnp.float32)).astype(
        jnp.bfloat16
    )
    for s in range(parts):
        at = slice(s * piece, (s + 1) * piece)
        gw_ref[at, :] = term(z, s)
    for k in range(1, nz):
        q_copy(k).wait_recv()
        z_copy(1, k).wait_recv()
    for t in range(nz):
        for s in range(parts):
            at = slice(s * piece, (s + 1) * piece)
            if t > 0:
                @pl.when(z == t)
                def _():
                    line_copy(True, t, s).wait_recv()
                    gw_ref[at, :] += up_recv[t, s].astype(jnp.float32)
            if t < nz - 1:
                @pl.when(z == t)
                def _():
                    line_copy(False, t, s).wait_recv()
                    gw_ref[at, :] += down_recv[t, s].astype(jnp.float32)
    for up, t in hops:
        for s in range(parts):
            @pl.when((z < t) if up else (z > t))
            def _():
                line_copy(up, t, s).wait_send()
    for k in range(1, nz):
        for part in range(5):
            send(part, k).wait_send()
        q_copy(k).wait_send()
        for part in range(2):
            z_copy(part, k).wait_send()
    for k in range(nz):
        lat_copy(k).wait_send()
        home_copy(k).wait_send()
        for part in range(2):
            passed(part, k).wait_send()
            y_copy(part, k).wait_send()
    for bit, leaving, _ in moves:
        for o in leaving:
            side_copy(bit, o).wait_send()


def level_call(
    queries, keys, latents, value_weight, first, second, cotangent, lse, head_lambda, n, ntp
):
    rows = queries.shape[0]
    depth, wide = value_weight.shape
    nz = n // 2
    width, share = depth // n, depth // ntp
    parts = 2 if width % 256 == 0 else 1
    dense, exact = jnp.bfloat16, jnp.float32
    vmem = pl.BlockSpec(memory_space=pltpu.VMEM)
    hbm = pl.BlockSpec(memory_space=pl.ANY)
    sem = pltpu.SemaphoreType.DMA
    buffers = (
        [((rows, wide), dense)] * 3
        + [((rows, depth), dense), ((depth, wide), dense)]
        + [((rows, wide), dense), ((nz, 8, rows), exact), ((rows, wide), dense)]
        + [((nz, rows, DV), dense)] * 2
        + [((n * rows, DV), dense)] * 2
        + [((nz, 8, rows), exact)]
        + [((n * rows, DV), dense)] * 2
        + [((nz, rows, width), dense), ((2 * rows, DV), dense), ((4, rows, BLOCK), exact)]
        + [((rows, DV), exact), ((nz, rows, DV), dense)]
        + [((DV, n * rows), exact)] * 2
        + [((n * rows, DV), exact)] * 2
        + [((nz, rows, DV), dense)] * 6
        + [((2 * rows, wide), dense)]
        + [((ntp, rows, share), dense)] * 2
        + [((nz, parts, width // parts, wide), dense)] * 4
        + [((width // parts, wide), exact)]
    )
    sems = (
        [(5,), (4,), (5, nz), (5, nz), (2, nz), (2, nz), (nz,), (nz,)]
        + [(nz,), (nz,), (2, nz), (2, nz), (2, nz), (2, nz), (nz,), (nz,), (ntp,), (ntp,)]
        + [(nz, parts)] * 4
    )
    return pl.pallas_call(
        functools.partial(level_kernel, nz, ntp),
        out_shape=[
            jax.ShapeDtypeStruct((rows, wide), dense),
            jax.ShapeDtypeStruct((rows, wide), dense),
            jax.ShapeDtypeStruct((rows, share), dense),
            jax.ShapeDtypeStruct((width, wide), exact),
        ],
        in_specs=[hbm] * 7 + [vmem, pl.BlockSpec(memory_space=pltpu.SMEM)],
        out_specs=[vmem] * 4,
        scratch_shapes=[pltpu.VMEM(*b) for b in buffers] + [sem(s) for s in sems],
        compiler_params=pltpu.CompilerParams(collective_id=1, has_side_effects=True),
    )(queries, keys, latents, value_weight, first, second, cotangent, lse, head_lambda)


def finish_kernel(q_ref, k_ref, gl_ref, gw_ref, q_out, k_out, gl_out, gw_out):
    q_out[...] = q_ref[...].astype(jnp.float32)
    k_out[...] = k_ref[...].astype(jnp.float32)
    gl_out[...] = gl_ref[...]
    gw_out[...] = gw_ref[...]


def finish(q_home, k_home, gl, gw):
    vmem = pl.BlockSpec(memory_space=pltpu.VMEM)
    kinds = ((q_home, jnp.float32), (k_home, jnp.float32), (gl, gl.dtype), (gw, gw.dtype))
    return pl.pallas_call(
        finish_kernel,
        out_shape=[jax.ShapeDtypeStruct(a.shape, kind) for a, kind in kinds],
        in_specs=[vmem] * 4,
        out_specs=[vmem] * 4,
    )(q_home, k_home, gl, gw)


def by_level(
    queries, key_vectors, latents, value_weight, log_sums, out_first, out_second, cotangent,
    head_lambda
):
    n, ntp = lax.axis_size("sp"), lax.axis_size("tp")
    return tuple(
        finish(
            *level_call(
                queries, key_vectors, latents, value_weight, out_first, out_second, cotangent,
                log_sums.T, head_lambda, n, ntp
            )
        )
    )


def dispatch(queries, key_vectors, latents, value_weight, log_sums, *rest):
    n, ntp = lax.axis_size("sp"), lax.axis_size("tp")
    rows, depth = latents.shape
    heads = rest[-1].shape[0]
    fits = heads * 2 == n and heads & (heads - 1) == 0 and heads > 1
    fits = fits and ntp & (ntp - 1) == 0 and ntp > 1
    fits = fits and rows % 32 == 0 and (n * rows) % BLOCK == 0
    fits = fits and depth % (n * DV) == 0 and depth % (ntp * DV) == 0
    fits = fits and depth // ntp == value_weight.shape[1]
    run = by_level if fits else per_device
    return run(queries, key_vectors, latents, value_weight, log_sums, *rest)


def solution(mesh):
    return jax.shard_map(
        dispatch,
        mesh=mesh,
        in_specs=(
            P("sp", "tp"),
            P("sp", "tp"),
            P("sp", None),
            P(None, "tp"),
            P("sp", "tp"),
            P("sp", "tp"),
            P("sp", "tp"),
            P("sp", "tp"),
            P("tp"),
        ),
        out_specs=(P("sp", "tp"), P("sp", "tp"), P("sp", "tp"), P("sp", "tp")),
        check_vma=False,
    )
```

time: 104 us -> 90.3 us (0.87)
  Pallas kernels: 103 us -> 88.9 us
    pallas_call x2 -> x1, Pallas kernels: 100 us -> 86.3 us  [level_call(): pl.pallas_call(functools.partial(level_kernel, nz, ntp), out_shape=[jax.S...]
where the time goes in v2:
time: 90.3 us; the launch traced here: 89.5 us
  Pallas kernels  88.9 us (98%)
    pallas_call x1, Pallas kernels, level_call(): pl.pallas_call(functools.partial(level_kernel, nz, ntp), out_shape=[jax.S...  86.3 us
    pallas_call x1, Pallas kernels, finish(): pl.pallas_call(finish_kernel, out_shape=[jax.ShapeDtypeStruct(a.shape, ki...  2.63 us

profile of v2, /device:TPU:0, one launch (start us, length us, event | category | flops | bytes accessed | tf_op | source)
XLA Modules:
  0.0 89.5 jit_solution(3323917430622933362)
XLA Ops:
  0.6 86.3 %shard_map.120 = (bf16[288,512]{1,0:T(8,128)(2,1)}, bf16[288,512]{1,0:T(8,128)(2,1)}, bf16[288,512]{1,0:T(8,128)(2,1)}, f32[256,512]{1,0:T(8,128)}) custom-call(bf16[288,512]{1,0:T(8,128)(2,1)} %q_ref.1, bf16[288,512]{1,0:T(8,128)(2,1)} %k_ref.1, bf16[288,2048]{1,0:T(8,128)(2,1)} %lat_ref.1, bf16[2048,512]{1,0:T(8,128)(2,1)} %w_ref.1, ...), custom_call_target="tpu_custom_call" | custom-call | tf_op jit(solution)/shard_map/pallas_call | solution.py:607
  86.9 2.6 %shard_map.121 = (f32[288,512]{1,0:T(8,128)}, f32[288,512]{1,0:T(8,128)}, bf16[288,512]{1,0:T(8,128)(2,1)}, f32[256,512]{1,0:T(8,128)}) custom-call(bf16[288,512]{1,0:T(8,128)(2,1)} %get-tuple-element.8.q_ref, bf16[288,512]{1,0:T(8,128)(2,1)} %get-tuple-element.9.k_ref, bf16[288,512]{1,0:T(8,128)(2,1)} %get-tuple-element.10.gl_ref, ...), custom_call_target="tpu_custom_call" | custom-call | tf_op jit(solution)/shard_map/pallas_call | solution.py:632

commit v3 on v2

--- a/solution.py
+++ b/solution.py
@@ -201,12 +201,12 @@
     nz, ntp, q_ref, k_ref, lat_ref, w_ref, first_ref, second_ref, cot_ref, lse_ref, lambda_ref,
     q_home, k_home, gl_ref, gw_ref,
     first_s, second_s, cot_s, lat_s, w_s, grad_s, stat_s, v_s, q_all, do_all, k_all, v_all,
-    stat_r, k0_s, k1_s, latp_s, qq_s, wide_s, dq_acc, dq_s, dkt_s, dvt_s, dk_s, dv_s,
-    dko_s, dvo_s, dky_s, dvy_s, dks_s, dvs_s, v_pair, gl_s, gl_recv,
-    up_send, up_recv, down_send, down_recv, sum_s,
+    stat_r, stat_t, q0_s, q1_s, latp_s, kk_s, s0_s, s1_s, a0_s, a1_s, dk_acc, dv_acc, dqt_s, dq_s,
+    dqo_s, dqy_s, dqs_s, dks_s, dvs_s, v_pair, gl_s, gl_recv,
+    line_send, line_recv, sum_s,
     load_sem, own_sem, send_sem, recv_sem, pass_send, pass_recv, lat_send, lat_recv,
-    q_send, q_recv, y_send, y_recv, z_send, z_recv, h_send, h_recv, t_send, t_recv,
-    u_send, u_recv, d_send, d_recv
+    y_send, y_recv, z_send, z_recv, h_send, h_recv, t_send, t_recv,
+    u_send, u_recv
 ):
     sp, tp = lax.axis_index("sp"), lax.axis_index("tp")
     z, y = sp // 2, lax.rem(sp, 2)
@@ -219,37 +219,38 @@
     loads = [
         pltpu.make_async_copy(src, dst, load_sem.at[i])
         for i, (src, dst) in enumerate(
-            [(lat_ref, lat_s), (w_ref, w_s), (first_ref, first_s), (second_ref, second_s),
-             (cot_ref, cot_s)]
+            [(first_ref, first_s), (second_ref, second_s), (cot_ref, cot_s), (lat_ref, lat_s),
+             (w_ref, w_s)]
         )
     ]
     for load in loads:
         load.start()
     arrived = greet(peers + [partner] + list(sides.values()))
-    own_q = pltpu.make_async_copy(q_ref.at[:, lanes(z)], q_all.at[z], own_sem.at[0])
-    own_k = pltpu.make_async_copy(k_ref.at[:, lanes(z)], k_all.at[chunk(sp, rows)], own_sem.at[1])
+    own_q = pltpu.make_async_copy(
+        q_ref.at[:, lanes(z)], q_all.at[chunk(sp, rows)], own_sem.at[0]
+    )
+    own_k = pltpu.make_async_copy(k_ref.at[:, lanes(z)], k_all.at[z], own_sem.at[1])
     own_q.start()
     own_k.start()
-    dkt_s[...] = jnp.zeros_like(dkt_s)
-    dvt_s[...] = jnp.zeros_like(dvt_s)
+    dqt_s[...] = jnp.zeros_like(dqt_s)
     arrived()
 
     def send(part, k):
         to = level(z, k, nz)
         src, dst = {
-            0: (q_ref.at[:, lanes(to)], q_all.at[z]),
-            1: (grad_s.at[:, lanes(to)], do_all.at[z]),
-            2: (stat_s.at[to], stat_r.at[z]),
-            3: (k_ref.at[:, lanes(to)], k_all.at[chunk(sp, rows)]),
-            4: (v_s.at[:, lanes(to)], v_all.at[chunk(sp, rows)]),
+            0: (q_ref.at[:, lanes(to)], q_all.at[chunk(sp, rows)]),
+            1: (grad_s.at[:, lanes(to)], do_all.at[chunk(sp, rows)]),
+            2: (stat_s.at[to], stat_r.at[sp]),
+            3: (k_ref.at[:, lanes(to)], k_all.at[z]),
+            4: (v_s.at[:, lanes(to)], v_all.at[z]),
         }[part]
         return remote(src, dst, send_sem.at[part, k], recv_sem.at[part, k], peers[k - 1])
 
     def passed(part, k, own=None):
-        kept = (k_all, v_all)[part]
-        at = chunk(2 * level(z, k, nz) + y, rows)
-        src = kept.at[at] if own is None else own
-        return remote(src, kept.at[at], pass_send.at[part, k], pass_recv.at[part, k], partner)
+        at = 2 * level(z, k, nz) + y
+        kept = (q_all, do_all, stat_r)[part].at[at if part == 2 else chunk(at, rows)]
+        src = kept if own is None else own
+        return remote(src, kept, pass_send.at[part, k], pass_recv.at[part, k], partner)
 
     def lat_copy(t):
         return remote(
@@ -258,19 +259,9 @@
         )
 
     for k in range(1, nz):
-        send(3, k).start()
-    passed(0, 0, k_ref.at[:, lanes(z)]).start()
-    for load in loads[:2]:
-        load.wait()
-    v_s[...] = jnp.dot(lat_s[...], w_s[...], preferred_element_type=jnp.float32).astype(
-        jnp.bfloat16
-    )
-    for k in range(1, nz):
-        send(4, k).start()
-    passed(1, 0, v_s.at[:, lanes(z)]).start()
-    own_v = pltpu.make_async_copy(v_s.at[:, lanes(z)], v_all.at[chunk(sp, rows)], own_sem.at[2])
-    own_v.start()
-    for load in loads[2:]:
+        send(0, k).start()
+    passed(0, 0, q_ref.at[:, lanes(z)]).start()
+    for load in loads[:3]:
         load.wait()
     columns = []
     for head in range(nz):
@@ -294,115 +285,52 @@
             [lse_ref[pair, :], dots[pair, :], jnp.zeros((4, rows), jnp.float32)], axis=0
         )
     for k in range(1, nz):
-        for part in (2, 0, 1):
+        for part in (2, 1):
             send(part, k).start()
-    own_do = pltpu.make_async_copy(grad_s.at[:, lanes(z)], do_all.at[z], own_sem.at[3])
+    passed(2, 0, stat_s.at[z]).start()
+    passed(1, 0, grad_s.at[:, lanes(z)]).start()
+    own_do = pltpu.make_async_copy(
+        grad_s.at[:, lanes(z)], do_all.at[chunk(sp, rows)], own_sem.at[2]
+    )
     own_do.start()
-    stat_r[z] = stat_s[z]
-
-    for part in (3, 4):
+    stat_r[sp] = stat_s[z]
+    for load in loads[3:]:
+        load.wait()
+    v_s[...] = jnp.dot(lat_s[...], w_s[...], preferred_element_type=jnp.float32).astype(
+        jnp.bfloat16
+    )
+    for k in range(1, nz):
+        for part in (3, 4):
+            send(part, k).start()
+    own_v = pltpu.make_async_copy(v_s.at[:, lanes(z)], v_all.at[z], own_sem.at[3])
+    own_v.start()
+    for part in (0, 2, 1):
         for k in range(1, nz):
             send(part, k).wait_recv()
-            passed(part - 3, k).start()
+            passed(part, k).start()
     for t in range(nz):
         lat_copy(t).start()
-    own_k.wait()
-    own_v.wait()
-    for part in range(2):
+    own_q.wait()
+    own_do.wait()
+    for part in range(3):
         for k in range(nz):
             passed(part, k).wait_recv()
-    keys = k_all[...]
-    half = lax.broadcasted_iota(jnp.int32, keys.shape, 1) < DH
-    k0_s[...] = jnp.where(half, keys, jnp.zeros_like(keys))
-    k1_s[...] = jnp.where(half, jnp.zeros_like(keys), keys)
+    scale = jnp.bfloat16(DH**-0.5)
+    queries = q_all[...] * scale
+    half = lax.broadcasted_iota(jnp.int32, queries.shape, 1) < DH
+    q0_s[...] = jnp.where(half, queries, jnp.zeros_like(queries))
+    q1_s[...] = jnp.where(half, jnp.zeros_like(queries), queries)
+    tiles = stat_t.shape[0]
+    stats = jnp.concatenate([stat_r[c] for c in range(2 * nz)], axis=1)
+    for t in range(tiles):
+        stat_t[t] = stats[:, t * BLOCK : (t + 1) * BLOCK]
     weight = lambda_ref[z]
-    scale = jnp.bfloat16(DH**-0.5)
-
-    def q_copy(k):
-        return remote(
-            dq_s.at[k], q_home.at[:, lanes(z)], q_send.at[k], q_recv.at[k], peers[k - 1]
-        )
-
-    for k in range(nz):
-        at = level(z, k, nz)
-        if k == 0:
-            own_q.wait()
-            own_do.wait()
-        else:
-            for part in range(3):
-                send(part, k).wait_recv()
-        queries = q_all[at] * scale
-        left = lax.broadcasted_iota(jnp.int32, queries.shape, 1) < DH
-        qq_s[0:rows, :] = jnp.where(left, queries, jnp.zeros_like(queries))
-        qq_s[rows:, :] = jnp.where(left, jnp.zeros_like(queries), queries)
-        queries_t = queries.T
-        grads_t = do_all[at].T
-        stats = stat_r[at].T
-        for i in range(4):
-            wide_s[i] = jnp.broadcast_to(stats[:, i : i + 1], (rows, BLOCK))
-        dq_acc[...] = jnp.zeros_like(dq_acc)
-        place = 2 * at + y
-        full = (place * rows + 1) // BLOCK
-        end = ((place + 1) * rows - 1) // BLOCK + 1
-
-        def tile(t, masked):
-            key_rows = chunk(t, BLOCK)
-            s01 = lax.dot_general(
-                qq_s[...], k_all[key_rows, :], NT, preferred_element_type=jnp.float32
-            )
-            d_attn = lax.dot_general(
-                do_all[at], v_all[key_rows, :], NT, preferred_element_type=jnp.float32
-            )
-            x0 = s01[:rows] - wide_s[0]
-            x1 = s01[rows:] - wide_s[1]
-            if masked:
-                key_at = lax.broadcasted_iota(jnp.int32, (rows, BLOCK), 1) + t * BLOCK
-                query_at = lax.broadcasted_iota(jnp.int32, (rows, BLOCK), 0) + place * rows
-                x0 = jnp.where(key_at <= query_at, x0, -1e30)
-                x1 = jnp.where(key_at <= query_at, x1, -1e30)
-            p0 = jnp.exp(x0)
-            p1 = weight * jnp.exp(x1)
-            ds0 = (p0 * (d_attn - wide_s[2])).astype(jnp.bfloat16)
-            ds1 = (p1 * (wide_s[3] - d_attn)).astype(jnp.bfloat16)
-            w = (p0 - p1).astype(jnp.bfloat16)
-            dq_acc[...] += jnp.dot(
-                ds0, k0_s[key_rows, :], preferred_element_type=jnp.float32
-            ) + jnp.dot(ds1, k1_s[key_rows, :], preferred_element_type=jnp.float32)
-            columns = lanes(t, BLOCK)
-            dkt_s[:DH, columns] += jnp.dot(
-                queries_t[:DH], ds0, preferred_element_type=jnp.float32
-            )
-            dkt_s[DH:, columns] += jnp.dot(
-                queries_t[DH:], ds1, preferred_element_type=jnp.float32
-            )
-            dvt_s[:, columns] += jnp.dot(grads_t, w, preferred_element_type=jnp.float32)
-
-        def full_tiles(t, carry):
-            tile(t, False)
-            return carry
-
-        def edge_tiles(t, carry):
-            tile(t, True)
-            return carry
-
-        lax.fori_loop(0, full, full_tiles, 0)
-        lax.fori_loop(full, end, edge_tiles, 0)
-        grad_q = (dq_acc[...] * DH ** (-0.5)).astype(jnp.bfloat16)
-        if k == 0:
-            q_home[:, lanes(z)] = grad_q
-        else:
-            dq_s[k] = grad_q
-            q_copy(k).start()
-
-    def y_copy(part, k):
-        at = level(z, k, nz)
-        src, dst = ((dvo_s, dvy_s), (dko_s, dky_s))[part]
-        return remote(src.at[at], dst.at[at], y_send.at[part, k], y_recv.at[part, k], partner)
 
     def z_copy(part, k):
-        at = level(z, k, nz)
-        src = (dvs_s, dks_s)[part].at[at]
-        dst = v_pair.at[0:rows, lanes(z)] if part == 0 else k_home.at[:, lanes(z)]
+        src = (dvs_s, dks_s, dqs_s)[part].at[k]
+        dst = (
+            v_pair.at[0:rows, lanes(z)], k_home.at[:, lanes(z)], q_home.at[:, lanes(z)]
+        )[part]
         return remote(src, dst, z_send.at[part, k], z_recv.at[part, k], peers[k - 1])
 
     def home_copy(k):
@@ -412,31 +340,107 @@
             h_send.at[k], h_recv.at[k], partner
         )
 
+    for k in range(nz):
+        at = level(z, k, nz)
+        if k == 0:
+            own_k.wait()
+            own_v.wait()
+        else:
+            for part in (3, 4):
+                send(part, k).wait_recv()
+        keys = k_all[at]
+        keys_t = keys.T
+        keys = keys * scale
+        left = lax.broadcasted_iota(jnp.int32, keys.shape, 1) < DH
+        kk_s[0:rows, :] = jnp.where(left, keys, jnp.zeros_like(keys))
+        kk_s[rows:, :] = jnp.where(left, jnp.zeros_like(keys), keys)
+        dk_acc[...] = jnp.zeros_like(dk_acc)
+        dv_acc[...] = jnp.zeros_like(dv_acc)
+        place = 2 * at + y
+        begin = (place * rows) // BLOCK
+
+        def scores(t, held):
+            query_rows = chunk(t, BLOCK)
+            held[0][...] = lax.dot_general(
+                kk_s[...], q_all[query_rows, :], NT, preferred_element_type=jnp.float32
+            )
+            held[1][...] = lax.dot_general(
+                v_all[at], do_all[query_rows, :], NT, preferred_element_type=jnp.float32
+            )
+
+        def tile(t, held):
+            query_rows = chunk(t, BLOCK)
+            stat = stat_t[t]
+            d_attn = held[1][...]
+            key_at = lax.broadcasted_iota(jnp.int32, (rows, BLOCK), 0)
+            query_at = lax.broadcasted_iota(jnp.int32, (rows, BLOCK), 1)
+            seen = key_at - query_at <= t * BLOCK - place * rows
+            p0 = jnp.exp(jnp.where(seen, held[0][:rows, :] - stat[0:1, :], -1e30))
+            p1 = weight * jnp.exp(jnp.where(seen, held[0][rows:, :] - stat[1:2, :], -1e30))
+            ds0 = (p0 * (d_attn - stat[2:3, :])).astype(jnp.bfloat16)
+            ds1 = (p1 * (stat[3:4, :] - d_attn)).astype(jnp.bfloat16)
+            w = (p0 - p1).astype(jnp.bfloat16)
+            dk_acc[...] += jnp.dot(
+                ds0, q0_s[query_rows, :], preferred_element_type=jnp.float32
+            ) + jnp.dot(ds1, q1_s[query_rows, :], preferred_element_type=jnp.float32)
+            dv_acc[...] += jnp.dot(w, do_all[query_rows, :], preferred_element_type=jnp.float32)
+            columns = lanes(t, BLOCK)
+            dqt_s[:DH, columns] += jnp.dot(keys_t[:DH], ds0, preferred_element_type=jnp.float32)
+            dqt_s[DH:, columns] += jnp.dot(keys_t[DH:], ds1, preferred_element_type=jnp.float32)
+
+        even, odd = (s0_s, a0_s), (s1_s, a1_s)
+        scores(begin, even)
+
+        def pair(i, carry):
+            t = begin + 2 * i
+            scores(t + 1, odd)
+            tile(t, even)
+            scores(jnp.minimum(t + 2, tiles - 1), even)
+            tile(t + 1, odd)
+            return carry
+
+        lax.fori_loop(0, (tiles - begin) // 2, pair, 0)
+
+        @pl.when((tiles - begin) % 2 == 1)
+        def _():
+            tile(tiles - 1, even)
+
+        grad_v, grad_k = dv_acc[...].astype(jnp.bfloat16), dk_acc[...].astype(jnp.bfloat16)
+        if k == 0:
+            v_pair[0:rows, lanes(z)] = grad_v
+            k_home[:, lanes(z)] = grad_k
+            home_copy(0).start()
+        else:
+            dvs_s[k] = grad_v
+            z_copy(0, k).start()
+            dks_s[k] = grad_k
+            z_copy(1, k).start()
+
+    def y_copy(k):
+        at = level(z, k, nz)
+        return remote(dqo_s.at[at], dqy_s.at[at], y_send.at[k], y_recv.at[k], partner)
+
     order = list(range(1, nz)) + [0]
-    for part, (turned, flat, other) in enumerate(((dvt_s, dv_s, dvo_s), (dkt_s, dk_s, dko_s))):
-        for t in range(flat.shape[0] // BLOCK):
-            at = slice(t * BLOCK, (t + 1) * BLOCK)
-            flat[at, :] = turned[:, at].T
-        for k in order:
-            at = level(z, k, nz)
-            other[at] = flat[chunk(2 * at + 1 - y, rows), :].astype(jnp.bfloat16)
-            y_copy(part, k).start()
-    for part, (flat, got, total) in enumerate(((dv_s, dvy_s, dvs_s), (dk_s, dky_s, dks_s))):
-        for k in order:
-            at = level(z, k, nz)
-            y_copy(part, k).wait_recv()
-            added = flat[chunk(2 * at + y, rows), :] + got[at].astype(jnp.float32)
-            added = added.astype(jnp.bfloat16)
-            if k == 0:
-                if part == 0:
-                    v_pair[0:rows, lanes(z)] = added
-                else:
-                    k_home[:, lanes(z)] = added
-            else:
-                total[at] = added
-                z_copy(part, k).start()
-    home_copy(0).start()
-    for k in range(1, nz):
+    for t in range(tiles):
+        at = slice(t * BLOCK, (t + 1) * BLOCK)
+        dq_s[at, :] = (dqt_s[:, at] * DH ** (-0.5)).T
+    for k in order:
+        at = level(z, k, nz)
+        dqo_s[at] = dq_s[chunk(2 * at + 1 - y, rows), :].astype(jnp.bfloat16)
+        y_copy(k).start()
+    for k in range(1, nz - 1):
+        z_copy(0, k).wait_recv()
+        home_copy(k).start()
+    for k in order:
+        at = level(z, k, nz)
+        y_copy(k).wait_recv()
+        added = dq_s[chunk(2 * at + y, rows), :] + dqy_s[at].astype(jnp.float32)
+        if k == 0:
+            q_home[:, lanes(z)] = added.astype(jnp.bfloat16)
+        else:
+            dqs_s[k] = added.astype(jnp.bfloat16)
+            z_copy(2, k).start()
+    for k in range(nz - 1, nz):
         z_copy(0, k).wait_recv()
         home_copy(k).start()
 
@@ -482,46 +486,53 @@
     for k in range(nz):
         home_copy(k).wait_recv()
 
-    parts = up_send.shape[1]
+    parts = line_send.shape[2]
     piece = width // parts
 
     def term(t, s):
-        at = pl.ds(pl.multiple_of((2 * t + y) * width + s * piece, piece), piece)
-        own = lat_s[:, at]
+        block = max(piece, DV)
+        skip = s * piece % block
+        at = pl.ds(pl.multiple_of((2 * t + y) * width + s * piece - skip, DV), block)
+        own = lat_s[:, at][:, skip : skip + piece]
         other = latp_s[t, :, s * piece : (s + 1) * piece]
         return lax.dot_general(
             jnp.concatenate([own, other], axis=0), v_pair[...], TN,
             preferred_element_type=jnp.float32,
         )
 
-    def line_copy(up, t, s):
-        if up:
-            return remote(
-                up_send.at[t, s], up_recv.at[t, s], u_send.at[t, s], u_recv.at[t, s],
-                {"sp": 2 * (z + 1) + y}
-            )
+    flip = z // (nz // 2)
+    zz = z + flip * (nz - 1 - 2 * z)
+
+    def line_copy(way, t, s):
         return remote(
-            down_send.at[t, s], down_recv.at[t, s], d_send.at[t, s], d_recv.at[t, s],
-            {"sp": 2 * (z - 1) + y}
+            line_send.at[way, t, s], line_recv.at[way, t, s],
+            u_send.at[way, t, s], u_recv.at[way, t, s],
+            {"sp": 2 * (z + 1 - 2 * way) + y}
         )
 
     hops = []
     for i in range(nz - 1):
-        hops += [(True, nz - 1 - i), (False, i)]
-
-    for up, t in hops:
+        hops += [(0, nz - 1 - i), (1, i)]
+    hops = [(back, t) for back, t in hops if t < nz // 2 - 1 or not back]
+
+    for back, tt in hops:
+        way = flip + back * (1 - 2 * flip)
+        t = tt + flip * (nz - 1 - 2 * tt)
         for s in range(parts):
-            @pl.when((z < t) if up else (z > t))
+            @pl.when((zz > tt) if back else (zz < tt))
             def _():
                 sum_s[...] = term(t, s)
 
-                @pl.when((z > 0) if up else (z < nz - 1))
-                def _():
-                    line_copy(up, t, s).wait_recv()
-                    sum_s[...] += (up_recv if up else down_recv)[t, s].astype(jnp.float32)
-
-                (up_send if up else down_send)[t, s] = sum_s[...].astype(jnp.bfloat16)
-                line_copy(up, t, s).start()
+                def more():
+                    line_copy(way, t, s).wait_recv()
+                    sum_s[...] += line_recv[way, t, s].astype(jnp.float32)
+
+                if back:
+                    more()
+                else:
+                    pl.when(zz > 0)(more)
+                line_send[way, t, s] = sum_s[...].astype(jnp.bfloat16)
+                line_copy(way, t, s).start()
 
     last = bits[-1]
     side_copy(last, last).wait_recv()
@@ -532,38 +543,33 @@
         at = slice(s * piece, (s + 1) * piece)
         gw_ref[at, :] = term(z, s)
     for k in range(1, nz):
-        q_copy(k).wait_recv()
         z_copy(1, k).wait_recv()
-    for t in range(nz):
+        z_copy(2, k).wait_recv()
+    for way in range(2):
+        @pl.when((z < nz - 1) if way else (z > 0))
+        def _():
+            for s in range(parts):
+                line_copy(way, z, s).wait_recv()
+                gw_ref[s * piece : (s + 1) * piece, :] += line_recv[way, z, s].astype(jnp.float32)
+
+    for back, tt in hops:
+        way = flip + back * (1 - 2 * flip)
+        t = tt + flip * (nz - 1 - 2 * tt)
         for s in range(parts):
-            at = slice(s * piece, (s + 1) * piece)
-            if t > 0:
-                @pl.when(z == t)
-                def _():
-                    line_copy(True, t, s).wait_recv()
-                    gw_ref[at, :] += up_recv[t, s].astype(jnp.float32)
-            if t < nz - 1:
-                @pl.when(z == t)
-                def _():
-                    line_copy(False, t, s).wait_recv()
-                    gw_ref[at, :] += down_recv[t, s].astype(jnp.float32)
-    for up, t in hops:
-        for s in range(parts):
-            @pl.when((z < t) if up else (z > t))
+            @pl.when((zz > tt) if back else (zz < tt))
             def _():
-                line_copy(up, t, s).wait_send()
+                line_copy(way, t, s).wait_send()
     for k in range(1, nz):
         for part in range(5):
             send(part, k).wait_send()
-        q_copy(k).wait_send()
-        for part in range(2):
+        for part in range(3):
             z_copy(part, k).wait_send()
     for k in range(nz):
         lat_copy(k).wait_send()
         home_copy(k).wait_send()
-        for part in range(2):
+        y_copy(k).wait_send()
+        for part in range(3):
             passed(part, k).wait_send()
-            y_copy(part, k).wait_send()
     for bit, leaving, _ in moves:
         for o in leaving:
             side_copy(bit, o).wait_send()
@@ -576,7 +582,7 @@
     depth, wide = value_weight.shape
     nz = n // 2
     width, share = depth // n, depth // ntp
-    parts = 2 if width % 256 == 0 else 1
+    parts = 4 if width % 256 == 0 else 2
     dense, exact = jnp.bfloat16, jnp.float32
     vmem = pl.BlockSpec(memory_space=pltpu.VMEM)
     hbm = pl.BlockSpec(memory_space=pl.ANY)
@@ -585,24 +591,25 @@
         [((rows, wide), dense)] * 3
         + [((rows, depth), dense), ((depth, wide), dense)]
         + [((rows, wide), dense), ((nz, 8, rows), exact), ((rows, wide), dense)]
+        + [((n * rows, DV), dense)] * 2
         + [((nz, rows, DV), dense)] * 2
+        + [((n, 8, rows), exact), ((n * rows // BLOCK, 8, BLOCK), exact)]
         + [((n * rows, DV), dense)] * 2
-        + [((nz, 8, rows), exact)]
-        + [((n * rows, DV), dense)] * 2
-        + [((nz, rows, width), dense), ((2 * rows, DV), dense), ((4, rows, BLOCK), exact)]
-        + [((rows, DV), exact), ((nz, rows, DV), dense)]
-        + [((DV, n * rows), exact)] * 2
-        + [((n * rows, DV), exact)] * 2
-        + [((nz, rows, DV), dense)] * 6
+        + [((nz, rows, width), dense), ((2 * rows, DV), dense)]
+        + [((2 * rows, BLOCK), exact)] * 2
+        + [((rows, BLOCK), exact)] * 2
+        + [((rows, DV), exact)] * 2
+        + [((DV, n * rows), exact), ((n * rows, DV), exact)]
+        + [((nz, rows, DV), dense)] * 5
         + [((2 * rows, wide), dense)]
         + [((ntp, rows, share), dense)] * 2
-        + [((nz, parts, width // parts, wide), dense)] * 4
+        + [((2, nz, parts, width // parts, wide), dense)] * 2
         + [((width // parts, wide), exact)]
     )
     sems = (
-        [(5,), (4,), (5, nz), (5, nz), (2, nz), (2, nz), (nz,), (nz,)]
-        + [(nz,), (nz,), (2, nz), (2, nz), (2, nz), (2, nz), (nz,), (nz,), (ntp,), (ntp,)]
-        + [(nz, parts)] * 4
+        [(5,), (4,), (5, nz), (5, nz), (3, nz), (3, nz), (nz,), (nz,)]
+        + [(nz,), (nz,), (3, nz), (3, nz), (nz,), (nz,), (ntp,), (ntp,)]
+        + [(2, nz, parts)] * 2
     )
     return pl.pallas_call(
         functools.partial(level_kernel, nz, ntp),

time: 90.3 us -> 74.3 us (0.82)
  Pallas kernels: 88.9 us -> 73.4 us
    pallas_call x1, Pallas kernels: 86.3 us -> 70.8 us  [level_call(): pl.pallas_call(functools.partial(level_kernel, nz, ntp), out_shape=[jax.S...]
where the time goes in v3:
time: 74.3 us; the launch traced here: 74.1 us
  Pallas kernels  73.4 us (99%)
    pallas_call x1, Pallas kernels, level_call(): pl.pallas_call(functools.partial(level_kernel, nz, ntp), out_shape=[jax.S...  70.8 us
    pallas_call x1, Pallas kernels, finish(): pl.pallas_call(finish_kernel, out_shape=[jax.ShapeDtypeStruct(a.shape, ki...  2.63 us

profile of v3, /device:TPU:0, one launch (start us, length us, event | category | flops | bytes accessed | tf_op | source)
XLA Modules:
  0.0 74.1 jit_solution(4166532370939243284)
XLA Ops:
  0.6 70.8 %shard_map.120 = (bf16[288,512]{1,0:T(8,128)(2,1)}, bf16[288,512]{1,0:T(8,128)(2,1)}, bf16[288,512]{1,0:T(8,128)(2,1)}, f32[256,512]{1,0:T(8,128)}) custom-call(bf16[288,512]{1,0:T(8,128)(2,1)} %q_ref.1, bf16[288,512]{1,0:T(8,128)(2,1)} %k_ref.1, bf16[288,2048]{1,0:T(8,128)(2,1)} %lat_ref.1, bf16[2048,512]{1,0:T(8,128)(2,1)} %w_ref.1, ...), custom_call_target="tpu_custom_call" | custom-call | tf_op jit(solution)/shard_map/pallas_call | solution.py:614
  71.4 2.6 %shard_map.121 = (f32[288,512]{1,0:T(8,128)}, f32[288,512]{1,0:T(8,128)}, bf16[288,512]{1,0:T(8,128)(2,1)}, f32[256,512]{1,0:T(8,128)}) custom-call(bf16[288,512]{1,0:T(8,128)(2,1)} %get-tuple-element.8.q_ref, bf16[288,512]{1,0:T(8,128)(2,1)} %get-tuple-element.9.k_ref, bf16[288,512]{1,0:T(8,128)(2,1)} %get-tuple-element.10.gl_ref, ...), custom_call_target="tpu_custom_call" | custom-call | tf_op jit(solution)/shard_map/pallas_call | solution.py:639

commit v4 on v3

--- a/solution.py
+++ b/solution.py
@@ -458,29 +458,26 @@
             gl_s.at[o], gl_recv.at[o], t_send.at[o], t_recv.at[o], sides[bit]
         )
 
-    alive = list(range(ntp))
-    moves = []
+    moves, alive = [], list(range(ntp))
     for bit in bits:
-        leaving = [o for o in alive if o & bit]
-        if bit == 1:
-            for o in leaving:
-                gl_s[o] = latent_term(o)
-                side_copy(bit, o).start()
-            alive = [o for o in alive if not o & bit]
-            for o in alive:
-                gl_s[o] = latent_term(o)
-        else:
+        moves.append((bit, [o for o in alive if o & bit]))
+        alive = [o for o in alive if not o & bit]
+    for o in moves[0][1]:
+        gl_s[o] = latent_term(o)
+        side_copy(1, o).start()
+    for o in range(0, ntp, 2):
+        gl_s[o] = latent_term(o)
+
+    def later_sides():
+        for (before, came), (bit, leaving) in zip(moves, moves[1:]):
+            for o in came:
+                side_copy(before, o).wait_recv()
+                gl_s[o - before] = (
+                    gl_s[o - before].astype(jnp.float32) + gl_recv[o].astype(jnp.float32)
+                ).astype(jnp.bfloat16)
             for o in leaving:
                 side_copy(bit, o).start()
-            alive = [o for o in alive if not o & bit]
-        moves.append((bit, leaving, alive))
-        if bit != bits[-1]:
-            for o in leaving:
-                side_copy(bit, o).wait_recv()
-            for o in alive:
-                gl_s[o] = (
-                    gl_s[o].astype(jnp.float32) + gl_recv[o + bit].astype(jnp.float32)
-                ).astype(jnp.bfloat16)
+
     for t in range(nz):
         lat_copy(t).wait_recv()
     for k in range(nz):
@@ -533,6 +530,9 @@
                     pl.when(zz > 0)(more)
                 line_send[way, t, s] = sum_s[...].astype(jnp.bfloat16)
                 line_copy(way, t, s).start()
+
+        if (back, tt) == hops[0]:
+            later_sides()
 
     last = bits[-1]
     side_copy(last, last).wait_recv()
@@ -570,7 +570,7 @@
         y_copy(k).wait_send()
         for part in range(3):
             passed(part, k).wait_send()
-    for bit, leaving, _ in moves:
+    for bit, leaving in moves:
         for o in leaving:
             side_copy(bit, o).wait_send()
 
@@ -626,21 +626,52 @@
     )(queries, keys, latents, value_weight, first, second, cotangent, lse, head_lambda)
 
 
-def finish_kernel(q_ref, k_ref, gl_ref, gw_ref, q_out, k_out, gl_out, gw_out):
-    q_out[...] = q_ref[...].astype(jnp.float32)
-    k_out[...] = k_ref[...].astype(jnp.float32)
-    gl_out[...] = gl_ref[...]
-    gw_out[...] = gw_ref[...]
+def finish_kernel(*refs):
+    ins, outs, held, wide, (in_sem, out_sem) = (
+        refs[:4], refs[4:8], refs[8:12], refs[12:14], refs[14:]
+    )
+
+    def halves(i):
+        rows = ins[i].shape[0] // 2
+        for h in range(2):
+            at = pl.ds(h * rows, rows)
+            source = wide[i] if i < 2 else held[i]
+            yield (
+                at,
+                pltpu.make_async_copy(ins[i].at[at], held[i].at[at], in_sem.at[i, h]),
+                pltpu.make_async_copy(source.at[at], outs[i].at[at], out_sem.at[i, h]),
+            )
+
+    copies = [list(halves(i)) for i in range(4)]
+    for group in copies:
+        for _, load, _ in group:
+            load.start()
+    for i, group in enumerate(copies):
+        for at, load, store in group:
+            load.wait()
+            if i < 2:
+                wide[i][at, :] = held[i][at, :].astype(jnp.float32)
+            store.start()
+    for group in copies:
+        for _, _, store in group:
+            store.wait()
 
 
 def finish(q_home, k_home, gl, gw):
-    vmem = pl.BlockSpec(memory_space=pltpu.VMEM)
-    kinds = ((q_home, jnp.float32), (k_home, jnp.float32), (gl, gl.dtype), (gw, gw.dtype))
+    hbm = pl.BlockSpec(memory_space=pl.ANY)
+    arrays = (q_home, k_home, gl, gw)
+    exact = [pltpu.VMEM(a.shape, jnp.float32) for a in arrays[:2]]
     return pl.pallas_call(
         finish_kernel,
-        out_shape=[jax.ShapeDtypeStruct(a.shape, kind) for a, kind in kinds],
-        in_specs=[vmem] * 4,
-        out_specs=[vmem] * 4,
+        out_shape=[
+            jax.ShapeDtypeStruct(a.shape, kind)
+            for a, kind in zip(arrays, (jnp.float32, jnp.float32, gl.dtype, gw.dtype))
+        ],
+        in_specs=[hbm] * 4,
+        out_specs=[hbm] * 4,
+        scratch_shapes=[pltpu.VMEM(a.shape, a.dtype) for a in arrays]
+        + exact
+        + [pltpu.SemaphoreType.DMA((4, 2))] * 2,
     )(q_home, k_home, gl, gw)
 
 

time: 74.3 us -> 74 us (level)
  the two profiles are of different devices: /device:TPU:0 before, /device:TPU:8 now
where the time goes in v4:
time: 74 us; the launch traced here: 73.7 us
  Pallas kernels  73.1 us (99%)
    pallas_call x1, Pallas kernels, level_call(): pl.pallas_call(functools.partial(level_kernel, nz, ntp), out_shape=[jax.S...  70.7 us
    pallas_call x1, Pallas kernels, finish(): pl.pallas_call(finish_kernel, out_shape=[jax.ShapeDtypeStruct(a.shape, ki...  2.35 us

profile of v4, /device:TPU:8, one launch (start us, length us, event | category | flops | bytes accessed | tf_op | source)
XLA Modules:
  0.0 73.7 jit_solution(17017053170006310915)
XLA Ops:
  0.6 70.7 %shard_map.120 = (bf16[288,512]{1,0:T(8,128)(2,1)}, bf16[288,512]{1,0:T(8,128)(2,1)}, bf16[288,512]{1,0:T(8,128)(2,1)}, f32[256,512]{1,0:T(8,128)}) custom-call(bf16[288,512]{1,0:T(8,128)(2,1)} %q_ref.1, bf16[288,512]{1,0:T(8,128)(2,1)} %k_ref.1, bf16[288,2048]{1,0:T(8,128)(2,1)} %lat_ref.1, bf16[2048,512]{1,0:T(8,128)(2,1)} %w_ref.1, ...), custom_call_target="tpu_custom_call" | custom-call | tf_op jit(solution)/shard_map/pallas_call | solution.py:614
  71.4 2.3 %shard_map.121 = (f32[288,512]{1,0:T(8,128)}, f32[288,512]{1,0:T(8,128)}, bf16[288,512]{1,0:T(8,128)(2,1)}, f32[256,512]{1,0:T(8,128)}) custom-call(bf16[288,512]{1,0:T(8,128)(2,1)} %get-tuple-element.8.refs_0_, bf16[288,512]{1,0:T(8,128)(2,1)} %get-tuple-element.9.refs_1_, bf16[288,512]{1,0:T(8,128)(2,1)} %get-tuple-element.10.refs_2_, ...), custom_call_target="tpu_custom_call" | custom-call | tf_op jit(solution)/shard_map/pallas_call | solution.py:664
